TPU v7x, 512 devices: a 4x2x32 block of a 4x8x32 slice. The times are simulated.
512 devices in a mesh: grp: 2 (over y), sp: 32 (over z), tp: 8 (over x, core).
Axes of the slice: x: 4, y: 2, z: 32, core: 2. Of those that a mesh axis runs over, the one named last changes fastest.
The devices are a block of a 4x8x32 slice.
Arguments:
- window_query: bfloat16 [20480, 2048], P(('grp', 'sp'), 'tp'), parts along dimension 0, may hold values from -24 to 24
- window_key: bfloat16 [20480, 1024], P(('grp', 'sp'), 'tp'), parts along dimension 0, may hold values from -24 to 24
- window_value: bfloat16 [20480, 1024], P(('grp', 'sp'), 'tp'), parts along dimension 0, may hold values from -6 to 6
- grid_query: bfloat16 [20480, 2048], P(('grp', 'sp'), 'tp'), parts along dimension 0, may hold values from -10 to 10
- grid_key: bfloat16 [20480, 1024], P(('grp', 'sp'), 'tp'), parts along dimension 0, may hold values from -10 to 10
- grid_value: bfloat16 [20480, 1024], P(('grp', 'sp'), 'tp'), parts along dimension 0, may hold values from -6 to 6
- sink_logit: float32 [16], P('tp'), may hold values from 1 to 6
- query_gain: float32 [128], replicated, may hold values from 0.8 to 6
- key_gain: float32 [128], replicated, may hold values from 0.8 to 6
- window_weights: bfloat16 [2048, 4096], P('tp'), may hold values from -0.59765625 to 0.59765625
- grid_weights: bfloat16 [2048, 4096], P('tp'), may hold values from -0.59765625 to 0.59765625
Outputs:
- merged: bfloat16 [20480, 4096], P(('grp', 'sp', 'tp')), parts along dimension 0
There are 2 independent parts, one for each index of `grp`. A program takes and returns all parts, laid end to end along the dimension named above; an argument that names none is the same for every part. Nothing has to cross between parts.
All inputs are finite; a program needn't handle non-finite values.
Results may differ from a plain program's by a relative error of at most 0.014.
The roundings to bfloat16 on the way count: a program that leaves them out, or rounds other values in their place, can miss the bound.
Values may be sent and summed in bfloat16 or wider, within the bound.
No kernel may reach another device: no remote copies, remote signals or barrier semaphores. Data moves between devices by JAX's collectives and lax.ppermute only.
A program may use at most 64 MiB of HBM per device.

v0:
```python
import functools
import math

import jax
import jax.numpy as jnp
from jax import lax
from jax.experimental import pallas as pl
from jax.experimental.pallas import tpu as pltpu
from jax.sharding import Mesh
from jax.sharding import PartitionSpec as P

HEAD = 128
QH_A = 16
WINDOW = 128
GRID_W = 64
THETA = 10000.0
NEGATIVE = -1e30
EPSILON = 1e-06
CORES = 2
PLANES = 4
TAIL = 32


def turn_tables(offset, local_rows):
    half = HEAD // 4
    frequency = THETA ** (-jnp.arange(0, HEAD // 2, 2, dtype=jnp.float32) / (HEAD // 2))
    places = offset + jnp.arange(local_rows, dtype=jnp.int32)
    row = (places // GRID_W).astype(jnp.float32)[:, None] * frequency[None, :]
    col = (places % GRID_W).astype(jnp.float32)[:, None] * frequency[None, :]
    angles = jnp.concatenate([row, row, col, col], axis=-1)
    lane = jnp.arange(HEAD, dtype=jnp.int32) % (2 * half)
    sign = jnp.where(lane < half, -1.0, 1.0).astype(jnp.float32)
    return jnp.cos(angles), jnp.sin(angles) * sign


def turn_kernel(x_ref, gain_ref, cos_ref, sin_ref, *rest):
    o_ref = rest[-1]
    width = x_ref.shape[1]
    lane = lax.broadcasted_iota(jnp.int32, (x_ref.shape[0], HEAD), 1) % (HEAD // 2)
    for k in range(width // HEAD):
        x = x_ref[:, k * HEAD : (k + 1) * HEAD].astype(jnp.float32)
        scaled = x * lax.rsqrt(jnp.mean(x * x, axis=-1, keepdims=True) + EPSILON)
        scaled = scaled * gain_ref[...]
        up = pltpu.roll(scaled, HEAD // 4, axis=1)
        down = pltpu.roll(scaled, HEAD - HEAD // 4, axis=1)
        other = jnp.where(lane < HEAD // 4, down, up)
        turned = scaled * cos_ref[...] + other * sin_ref[...]
        o_ref[:, k * HEAD : (k + 1) * HEAD] = turned.astype(jnp.bfloat16)
    if len(rest) == 2:
        o_ref[:, width:] = rest[0][...]


def turn(x, gain, cos, sin, beside=None):
    rows, width = x.shape
    args = [x, gain.reshape(1, HEAD), cos, sin]
    if beside is not None:
        args.append(beside)
        width = width + beside.shape[1]
    return pl.pallas_call(
        turn_kernel,
        out_shape=jax.ShapeDtypeStruct((rows, width), jnp.bfloat16),
        cost_estimate=pl.CostEstimate(
            flops=rows * width * 16, bytes_accessed=rows * width * 8, transcendentals=rows
        ),
    )(*args)


def attend_kernel(*refs, planes, pieces, last, chunk):
    first = planes > 1
    q_refs, refs = refs[:planes], refs[planes:]
    kv_refs, rest = refs[: len(pieces)], refs[len(pieces) :]
    factor = math.log2(math.e) * HEAD ** (-0.5)
    key_parts = [r[:, :HEAD] for r, kind in zip(kv_refs, pieces) if "k" in kind]
    value_parts = [r[:, r.shape[1] - HEAD :] for r, kind in zip(kv_refs, pieces) if "v" in kind]
    keys = jnp.concatenate(key_parts, axis=0)
    values = jnp.concatenate(value_parts, axis=0).T
    if first:
        before_refs = None
        q_ref = rest[3]
        count = q_refs[0].shape[0]
        for d in range(planes):
            q_ref[d * count : (d + 1) * count, :] = q_refs[d][...]
    else:
        q_ref = q_refs[0]
        before_refs, rest = rest[:3], rest[3:]
    rows = q_ref.shape[0]

    def score(lo):
        return lax.dot_general(
            keys,
            q_ref[lo : lo + chunk, :],
            (((1,), (1,)), ((), ())),
            preferred_element_type=jnp.float32,
        )

    def absorb(scores, lo):
        span = slice(lo, lo + chunk)
        top = jnp.max(scores, axis=0, keepdims=True)
        if not first:
            before = before_refs[0][:, span]
            top = jnp.maximum(before, top)
            fading = jnp.exp2((before - top) * factor)
        raised = jnp.exp2((scores - top) * factor)
        total = jnp.sum(raised, axis=0, keepdims=True)
        acc = lax.dot_general(
            values,
            raised.astype(jnp.bfloat16),
            (((1,), (0,)), ((), ())),
            preferred_element_type=jnp.float32,
        )
        if not first:
            total = total + before_refs[1][:, span] * fading
            acc = acc + before_refs[2][:, span] * fading
        if not last:
            rest[0][:, span] = top
            rest[1][:, span] = total
            rest[2][:, span] = acc
            return
        weight = top * factor + jnp.log2(total)
        high = weight.astype(jnp.bfloat16)
        left = weight - high.astype(jnp.float32)
        middle = left.astype(jnp.bfloat16)
        low = (left - middle.astype(jnp.float32)).astype(jnp.bfloat16)
        terms = [high, middle, low]
        tail = jnp.concatenate(
            [jnp.broadcast_to(t.astype(jnp.float32), (8, chunk)) for t in terms]
            + [jnp.zeros((8, chunk), jnp.float32)],
            axis=0,
        )
        out = (acc / total).astype(jnp.bfloat16)
        tail = tail.astype(jnp.bfloat16)
        each = rows // len(rest)
        for d in range(len(rest)):
            start, stop = max(lo, d * each), min(lo + chunk, (d + 1) * each)
            if start < stop:
                there = slice(start - d * each, stop - d * each)
                rest[d][:HEAD, there] = out[:, start - lo : stop - lo]
                rest[d][HEAD:, there] = tail[:, start - lo : stop - lo]

    waiting = None
    for lo in range(0, rows, chunk):
        scores = score(lo)
        if waiting is not None:
            absorb(*waiting)
        waiting = (scores, lo)
    absorb(*waiting)


def attend(queries, kvs, pieces, carry=None, parts=0, chunk=256):
    rows = sum(q.shape[0] for q in queries)
    while rows % chunk:
        chunk //= 2
    keys = sum(a.shape[0] for a, kind in zip(kvs, pieces) if "k" in kind)
    f32 = jnp.float32
    if parts:
        part = jax.ShapeDtypeStruct((HEAD + TAIL, rows // parts), jnp.bfloat16)
        out_shape = (part,) * parts
    else:
        out_shape = (
            jax.ShapeDtypeStruct((1, rows), f32),
            jax.ShapeDtypeStruct((1, rows), f32),
            jax.ShapeDtypeStruct((HEAD, rows), f32),
        )
    if carry is None:
        out_shape = out_shape + (jax.ShapeDtypeStruct((rows, HEAD), jnp.bfloat16),)
    return pl.pallas_call(
        functools.partial(
            attend_kernel, planes=len(queries), pieces=pieces, last=parts > 0, chunk=chunk
        ),
        out_shape=out_shape,
        cost_estimate=pl.CostEstimate(
            flops=4 * rows * keys * HEAD,
            bytes_accessed=rows * HEAD * 10,
            transcendentals=rows * keys,
        ),
    )(*queries, *kvs, *(carry or ()))


def merge_kernel(*refs):
    o_ref = refs[-1]
    heads = o_ref.shape[1] // HEAD
    count = o_ref.shape[0]
    parts = refs[:-1]
    weights = [
        r[HEAD : HEAD + 8, :].astype(jnp.float32)[:1]
        + r[HEAD + 8 : HEAD + 16, :].astype(jnp.float32)[:1]
        + r[HEAD + 16 : HEAD + 24, :].astype(jnp.float32)[:1]
        for r in parts
    ]
    top = functools.reduce(jnp.maximum, weights)
    shares = [jnp.exp2(w - top) for w in weights]
    total = functools.reduce(jnp.add, shares)
    out = functools.reduce(
        jnp.add, [r[:HEAD, :].astype(jnp.float32) * s for r, s in zip(parts, shares)]
    )
    out = (out / total).T.astype(jnp.bfloat16)
    for h in range(heads):
        o_ref[:, h * HEAD : (h + 1) * HEAD] = out[h * count : (h + 1) * count, :]


def grid_attend(kv, make_queries, heads, held):
    high = lax.axis_size("hi")
    low = lax.axis_size("lo")
    ring = [(i, (i + 1) % high) for i in range(high)]
    back = [(b, a) for a, b in ring]

    ahead = lax.ppermute(kv, "hi", ring)
    behind = lax.ppermute(kv, "hi", back)
    queries = make_queries(kv)
    shared = [queries] + [
        lax.ppermute(queries, "lo", [(i, (i + d) % low) for i in range(low)])
        for d in range(1, low)
    ]
    ahead, behind, held = lax.optimization_barrier((ahead, behind, held))
    rows, carry, waiting = shared, None, (kv,)
    for step in range(1, high // 2):
        if step + 1 < high // 2:
            next_ahead, next_behind = ahead, behind
        else:
            next_ahead, next_behind = ahead[:, :HEAD], behind[:, HEAD:]
        following = (lax.ppermute(next_ahead, "hi", ring), lax.ppermute(next_behind, "hi", back))
        blocks = waiting + (ahead, behind)
        result = attend(rows, blocks, ("kv",) * len(blocks), carry)
        carry, waiting = result[:3], ()
        if step == 1:
            rows = result[3:]
        ahead, behind = following
    parts = attend(rows, (ahead, behind), ("k", "v"), carry, parts=low)
    parts = [parts[0]] + [
        lax.ppermute(parts[d], "lo", [(i, (i - d) % low) for i in range(low)])
        for d in range(1, low)
    ]
    count = parts[0].shape[1]
    grid_out = pl.pallas_call(
        merge_kernel,
        out_shape=jax.ShapeDtypeStruct((count // heads, heads * HEAD), jnp.bfloat16),
        cost_estimate=pl.CostEstimate(
            flops=8 * count * HEAD, bytes_accessed=count * HEAD * 10, transcendentals=count
        ),
    )(*parts)
    return grid_out, held


def extended(cells, axes, width):
    count = math.prod(lax.axis_size(a) for a in axes)
    ends = count - 1
    head = cells[:, :width]
    tail = cells[:, cells.shape[1] - width :]
    above = lax.ppermute(tail, axes, [(i, i + 1) for i in range(ends)])
    below = lax.ppermute(head, axes, [(i + 1, i) for i in range(ends)])
    return jnp.concatenate([above, cells, below], axis=1)


def window_attend(queries, keys_pad, values_pad, slopes, sink_logits, offset, total_rows):
    query_rows = queries.shape[0]
    block_span = WINDOW // 2
    blocks = query_rows // block_span
    key_heads = keys_pad.shape[1] // HEAD
    group_size = queries.shape[1] // keys_pad.shape[1]
    query_blocks = queries.reshape(blocks, block_span, key_heads, group_size, HEAD)
    key_blocks = keys_pad.reshape(blocks + 4, block_span, key_heads, HEAD)
    value_blocks = values_pad.reshape(blocks + 4, block_span, key_heads, HEAD)
    key_window = jnp.concatenate([key_blocks[s : s + blocks] for s in range(5)], axis=1)
    value_window = jnp.concatenate([value_blocks[s : s + blocks] for s in range(5)], axis=1)
    scores = jnp.einsum(
        "nqkgd,nskd->kgnqs", query_blocks, key_window, preferred_element_type=jnp.float32
    ) * HEAD ** (-0.5)
    query_place = offset + jnp.arange(query_rows, dtype=jnp.int32).reshape(blocks, block_span, 1)
    key_place = (
        offset
        - WINDOW
        + block_span * jnp.arange(blocks, dtype=jnp.int32)[:, None, None]
        + jnp.arange(5 * block_span, dtype=jnp.int32)[None, None, :]
    )
    distance = jnp.abs(key_place - query_place)
    inside = (distance <= WINDOW) & (key_place >= 0) & (key_place < total_rows)
    slope_grid = slopes.reshape(key_heads, group_size, 1, 1, 1)
    sink_grid = sink_logits.reshape(key_heads, group_size, 1, 1)
    scores = jnp.where(inside, scores - slope_grid * distance.astype(jnp.float32), NEGATIVE)
    highest = jnp.maximum(jnp.max(scores, axis=-1), sink_grid)
    raised = jnp.exp(scores - highest[..., None])
    denominator = jnp.sum(raised, axis=-1) + jnp.exp(sink_grid - highest)
    weights = (raised / denominator[..., None]).astype(jnp.bfloat16)
    attended = jnp.einsum(
        "kgnqs,nskd->nqkgd", weights, value_window, preferred_element_type=jnp.float32
    )
    return attended.astype(jnp.bfloat16).reshape(query_rows, -1)


def by_target(rows):
    across = lax.axis_size("x")
    core = lax.axis_index("core")
    count = rows.shape[0] // (across * CORES)
    tiles = rows.reshape(across, CORES, count, rows.shape[1])
    tiles = jnp.where(core == 0, tiles, tiles[:, ::-1])
    return jnp.swapaxes(tiles, 0, 1).reshape(rows.shape)


def sent_and_summed(partial):
    half = partial.shape[0] // CORES
    across = lax.axis_size("x")
    theirs = lax.ppermute(partial[half:], "core", [(0, 1), (1, 0)])
    both = partial[:half].astype(jnp.float32) + theirs.astype(jnp.float32)
    tiles = both.astype(jnp.bfloat16).reshape(across, half // across, -1)
    tiles = lax.all_to_all(tiles, "x", 0, 0, tiled=True)
    return jnp.sum(tiles.astype(jnp.float32), axis=0)


def per_device(
    window_query,
    window_key,
    window_value,
    grid_query,
    grid_key,
    grid_value,
    sink_logit,
    query_gain,
    key_gain,
    window_weights,
    grid_weights,
):
    local_rows = window_query.shape[0]
    planes = ("hi", "lo")
    plane = lax.axis_index("hi") * PLANES + lax.axis_index("lo")
    head_group = lax.axis_index("x") * CORES + lax.axis_index("core")
    offset = plane * local_rows
    total_rows = local_rows * lax.axis_size("hi") * PLANES
    cos, sin = turn_tables(offset, local_rows)
    kv = turn(grid_key, key_gain, cos, sin, grid_value)
    heads = grid_query.shape[1] // HEAD

    def make_queries(after):
        _, given = lax.optimization_barrier((after, grid_query))
        turned = by_target(turn(given, query_gain, cos, sin))
        return jnp.concatenate(
            [turned[:, h * HEAD : (h + 1) * HEAD] for h in range(heads)], axis=0
        )

    grid_out, (window_query, window_key, window_value) = grid_attend(
        kv, make_queries, heads, (window_query, window_key, window_value)
    )

    local_heads = sink_logit.shape[0]
    head_number = head_group * local_heads + 1 + jnp.arange(local_heads, dtype=jnp.int32)
    slopes = 2.0 ** (-8.0 * head_number.astype(jnp.float32) / QH_A)
    padded = extended(jnp.stack([window_key, window_value]), planes, WINDOW)
    window_out = by_target(
        window_attend(window_query, padded[0], padded[1], slopes, sink_logit, offset, total_rows)
    )
    partial = jnp.dot(window_out, window_weights, preferred_element_type=jnp.float32) + jnp.dot(
        grid_out, grid_weights, preferred_element_type=jnp.float32
    )
    return sent_and_summed(partial.astype(jnp.bfloat16)).astype(jnp.bfloat16)


def solution(mesh):
    shape = mesh.shape
    inner = Mesh(
        mesh.devices.reshape(
            shape["grp"], shape["sp"] // PLANES, PLANES, shape["tp"] // CORES, CORES
        ),
        ("grp", "hi", "lo", "x", "core"),
    )
    rows = ("grp", "hi", "lo")
    heads = ("x", "core")

    return jax.shard_map(
        per_device,
        mesh=inner,
        in_specs=(
            P(rows, heads),
            P(rows, heads),
            P(rows, heads),
            P(rows, heads),
            P(rows, heads),
            P(rows, heads),
            P(heads),
            P(),
            P(),
            P(heads, None),
            P(heads, None),
        ),
        out_specs=P(rows + heads, None),
        check_vma=False,
    )
```

profile of v0, /device:TPU:33, one launch (start us, length us, event | category | flops | bytes accessed | tf_op | source)
XLA Modules:
  0.0 213.9 jit_solution(714165005102199191)
XLA Ops:
  0.2 1.4 sine_multiply_fusion
  1.7 2.0 shard_map.109.refs_4_
  3.7 2.2 %shard_map.110 = bf16[320,256]{1,0:T(8,128)(2,1)} custom-call(bf16[320,256]{1,0:T(8,128)(2,1)} %x_ref.2, f32[1,128]{1,0:T(1,128)} %bitcast.76, f32[320,128]{1,0:T(8,128)} %get-tuple-element.46.cos_ref, f32[320,128]{1,0:T(8,128)} %get-tuple-element.45.sin_ref), custom_call_target="tpu_custom_call" | custom-call | flops 1310720 | bytes 655360 | tf_op jit(solution)/shard_map/pallas_call | solution.py:59
  7.0 9.7 %collective-permute-start.6 = (bf16[640,128]{1,0:T(8,128)(2,1)S(1)}, bf16[640,128]{1,0:T(8,128)(2,1)}, u32[]{:S(2)}, u32[]{:S(2)}) collective-permute-start(bf16[640,128]{1,0:T(8,128)(2,1)S(1)} %pad_maximum_fusion.2.refs_0_), channel_id=1, source_target_pairs={{0,24},{8,0},{16,8},{24,16},{1,25},{9,1},{17,9},{25,17},{2,26},{10... | collective-permute-start | bytes 491528 | tf_op jit(solution)/shard_map/ppermute | solution.py:211
  16.7 2.0 collective-permute-start.5
  18.6 2.2 %collective-permute-start.4 = (bf16[640,128]{1,0:T(8,128)(2,1)S(1)}, bf16[640,128]{1,0:T(8,128)(2,1)}, u32[]{:S(2)}, u32[]{:S(2)}) collective-permute-start(bf16[640,128]{1,0:T(8,128)(2,1)S(1)} %pad_maximum_fusion.2.refs_0_), channel_id=1, source_target_pairs={{0,8},{8,16},{16,24},{24,0},{1,9},{9,17},{17,25},{25,1},{2,10},{10... | collective-permute-start | bytes 491528 | tf_op jit(solution)/shard_map/ppermute | solution.py:211
  20.9 41.1 %collective-permute-start.1 = (bf16[320,256]{1,0:T(8,128)(2,1)}, bf16[320,256]{1,0:T(8,128)(2,1)}, u32[]{:S(2)}, u32[]{:S(2)}) collective-permute-start(bf16[320,256]{1,0:T(8,128)(2,1)} %shard_map.109.refs_4_), channel_id=1, source_target_pairs={{32,0},{64,32},{96,64},{128,96},{160,128},{192,160},{224,192},{0,2... | collective-permute-start | bytes 491528 | tf_op jit(solution)/shard_map/ppermute | solution.py:208
  62.0 2.0 collective-permute-start
  64.6 8.1 %collective-permute-done.refs_5_ = bf16[320,256]{1,0:T(8,128)(2,1)} collective-permute-done((bf16[320,256]{1,0:T(8,128)(2,1)}, bf16[320,256]{1,0:T(8,128)(2,1)}, u32[]{:S(2)}, u32[]{:S(2)}) %collective-permute-start) | collective-permute-done | bytes 163872 | tf_op jit(solution)/shard_map/ppermute | solution.py:207
  73.3 1.3 collective-permute-start.3
  74.6 16.3 %collective-permute-start.2 = (bf16[2,128,128]{2,1,0:T(8,128)(2,1)}, bf16[2,128,128]{2,1,0:T(8,128)(2,1)S(1)}, u32[]{:S(2)}, u32[]{:S(2)}) collective-permute-start(bf16[2,128,128]{2,1,0:T(8,128)(2,1)} %get-tuple-element.60), channel_id=1, source_target_pairs={{0,8},{8,16},{16,24},{24,32},{32,40},{40,48},{48,56},{56,64},{64,7... | collective-permute-start | bytes 196616 | tf_op jit(solution)/shard_map/ppermute | solution.py:249
  91.1 3.1 %collective-permute-start.7 = (bf16[320,256]{1,0:T(8,128)(2,1)}, bf16[320,256]{1,0:T(8,128)(2,1)S(1)}, u32[]{:S(2)}, u32[]{:S(2)}) collective-permute-start(bf16[320,256]{1,0:T(8,128)(2,1)} %collective-permute-done.refs_5_), channel_id=1, source_target_pairs={{0,32},{32,64},{64,96},{96,128},{128,160},{160,192},{192,224},{224... | collective-permute-start | bytes 491528 | tf_op jit(solution)/shard_map/ppermute | solution.py:221
  94.2 6.2 %collective-permute-start.10 = (bf16[320,256]{1,0:T(8,128)(2,1)}, bf16[320,256]{1,0:T(8,128)(2,1)}, u32[]{:S(2)}, u32[]{:S(2)}) collective-permute-start(bf16[320,256]{1,0:T(8,128)(2,1)} %collective-permute-done.1.refs_6_), channel_id=1, source_target_pairs={{32,0},{64,32},{96,64},{128,96},{160,128},{192,160},{224,192},{0,2... | collective-permute-start | bytes 491528 | tf_op jit(solution)/shard_map/ppermute | solution.py:221
  100.4 6.3 %shard_map.111 = (f32[1,2560]{1,0:T(1,128)}, f32[1,2560]{1,0:T(1,128)}, f32[128,2560]{1,0:T(8,128)}, bf16[2560,128]{1,0:T(8,128)(2,1)}) custom-call(bf16[640,128]{1,0:T(8,128)(2,1)} %copy-done.7, bf16[640,128]{1,0:T(8,128)(2,1)} %collective-permute-done.4.refs_1_, bf16[640,128]{1,0:T(8,128)(2,1)} %collective-permute-done.5.refs_2_, ...), custom_call_target="tpu_custom_call" | custom-call | flops 1258291200 | bytes 3276800 | tf_op jit(solution)/shard_map/pallas_call | solution.py:166
  109.1 2.7 %collective-permute-start.8 = (bf16[320,256]{1,0:T(8,128)(2,1)S(1)}, bf16[320,256]{1,0:T(8,128)(2,1)S(1)}, u32[]{:S(2)}, u32[]{:S(2)}) collective-permute-start(bf16[320,256]{1,0:T(8,128)(2,1)S(1)} %collective-permute-done.7.refs_1_), channel_id=1, source_target_pairs={{0,32},{32,64},{64,96},{96,128},{128,160},{160,192},{192,224},{224... | collective-permute-start | bytes 491528 | tf_op jit(solution)/shard_map/ppermute | solution.py:221
  111.8 6.5 %collective-permute-start.11 = (bf16[320,256]{1,0:T(8,128)(2,1)}, bf16[320,256]{1,0:T(8,128)(2,1)S(1)}, u32[]{:S(2)}, u32[]{:S(2)}) collective-permute-start(bf16[320,256]{1,0:T(8,128)(2,1)} %collective-permute-done.10.refs_2_), channel_id=1, source_target_pairs={{32,0},{64,32},{96,64},{128,96},{160,128},{192,160},{224,192},{0,2... | collective-permute-start | bytes 491528 | tf_op jit(solution)/shard_map/ppermute | solution.py:221
  118.4 9.6 %collective-permute-done.8.refs_1_ = bf16[320,256]{1,0:T(8,128)(2,1)S(1)} collective-permute-done((bf16[320,256]{1,0:T(8,128)(2,1)S(1)}, bf16[320,256]{1,0:T(8,128)(2,1)S(1)}, u32[]{:S(2)}, u32[]{:S(2)}) %collective-permute-start.8) | collective-permute-done | bytes 163872 | tf_op jit(solution)/shard_map/ppermute | solution.py:221
  128.0 2.0 collective-permute-start.9
  130.0 7.5 %collective-permute-start.12 = (bf16[320,128]{1,0:T(8,128)(2,1)S(1)}, bf16[320,128]{1,0:T(8,128)(2,1)S(1)}, u32[]{:S(2)}, u32[]{:S(2)}) collective-permute-start(bf16[320,128]{1,0:T(8,128)(2,1)S(1)} %slice.139), channel_id=1, source_target_pairs={{32,0},{64,32},{96,64},{128,96},{160,128},{192,160},{224,192},{0,2... | collective-permute-start | bytes 245768 | tf_op jit(solution)/shard_map/ppermute | solution.py:221
  137.5 5.6 %shard_map.112 = (f32[1,2560]{1,0:T(1,128)}, f32[1,2560]{1,0:T(1,128)}, f32[128,2560]{1,0:T(8,128)}) custom-call(bf16[2560,128]{1,0:T(8,128)(2,1)} %get-tuple-element.31.refs_0_, bf16[320,256]{1,0:T(8,128)(2,1)} %copy-done.13, bf16[320,256]{1,0:T(8,128)(2,1)} %collective-permute-done.10.refs_2_, f32[1,2560]{1,0:T(1,128)} %get-tuple-element.32.refs_3_, ...), custom_call_target="tpu_custom_call" | custom-call | flops 838860800 | bytes 3276800 | tf_op jit(solution)/shard_map/pallas_call | solution.py:166
  143.1 5.6 %shard_map.113 = (f32[1,2560]{1,0:T(1,128)}, f32[1,2560]{1,0:T(1,128)}, f32[128,2560]{1,0:T(8,128)}) custom-call(bf16[2560,128]{1,0:T(8,128)(2,1)} %get-tuple-element.31.refs_0_, bf16[320,256]{1,0:T(8,128)(2,1)} %copy-done.10, bf16[320,256]{1,0:T(8,128)(2,1)} %copy-done.11, f32[1,2560]{1,0:T(1,128)} %get-tuple-element.35.refs_3_, ...), custom_call_target="tpu_custom_call" | custom-call | flops 838860800 | bytes 3276800 | tf_op jit(solution)/shard_map/pallas_call | solution.py:166
  149.3 4.1 %shard_map.114 = (bf16[160,640]{1,0:T(8,128)(2,1)}, bf16[160,640]{1,0:T(8,128)(2,1)}, bf16[160,640]{1,0:T(8,128)(2,1)}, bf16[160,640]{1,0:T(8,128)(2,1)}) custom-call(bf16[2560,128]{1,0:T(8,128)(2,1)} %get-tuple-element.31.refs_0_, bf16[320,128]{1,0:T(8,128)(2,1)} %copy-done.8, bf16[320,128]{1,0:T(8,128)(2,1)} %copy-done.9, ...), custom_call_target="tpu_custom_call" | custom-call | flops 419430400 | bytes 3276800 | tf_op jit(solution)/shard_map/pallas_call | solution.py:166
  153.5 6.0 %collective-permute-start.13 = (bf16[160,640]{1,0:T(8,128)(2,1)}, bf16[160,640]{1,0:T(8,128)(2,1)S(1)}, u32[]{:S(2)}, u32[]{:S(2)}) collective-permute-start(bf16[160,640]{1,0:T(8,128)(2,1)} %get-tuple-element.42), channel_id=1, source_target_pairs={{0,24},{8,0},{16,8},{24,16},{1,25},{9,1},{17,9},{25,17},{2,26},{10... | collective-permute-start | bytes 614408 | tf_op jit(solution)/shard_map/ppermute | solution.py:230
  159.5 3.8 %collective-permute-start.14 = (bf16[160,640]{1,0:T(8,128)(2,1)}, bf16[160,640]{1,0:T(8,128)(2,1)S(1)}, u32[]{:S(2)}, u32[]{:S(2)}) collective-permute-start(bf16[160,640]{1,0:T(8,128)(2,1)} %get-tuple-element.43), channel_id=1, source_target_pairs={{0,16},{8,24},{16,0},{24,8},{1,17},{9,25},{17,1},{25,9},{2,18},{10... | collective-permute-start | bytes 614408 | tf_op jit(solution)/shard_map/ppermute | solution.py:230
  163.3 2.0 collective-permute-start.15
  165.3 3.2 %fusion.28 = f32[320,4096]{1,0:T(8,128)} fusion(bf16[320,256]{1,0:T(8,128)(2,1)S(1)} %bitcast.58, bf16[256,4096]{1,0:T(8,128)(2,1)S(1)} %copy-done), kind=kOutput, calls=%fused_computation.72 | convolution fusion | flops 671088640 | bytes 7503872 | tf_op jit(solution)/shard_map/dot_general | solution.py:350
  168.4 10.3 %collective-permute-done.14.refs_2_ = bf16[160,640]{1,0:T(8,128)(2,1)S(1)} collective-permute-done((bf16[160,640]{1,0:T(8,128)(2,1)}, bf16[160,640]{1,0:T(8,128)(2,1)S(1)}, u32[]{:S(2)}, u32[]{:S(2)}) %collective-permute-start.14) | collective-permute-done | bytes 204832 | tf_op jit(solution)/shard_map/ppermute | solution.py:230
  179.5 2.1 shard_map.115
  181.6 4.0 %fusion = bf16[320,4096]{1,0:T(8,128)(2,1)S(1)} fusion(f32[320,4096]{1,0:T(8,128)} %fusion.28, bf16[320,256]{1,0:T(8,128)(2,1)} %shard_map.115, bf16[256,4096]{1,0:T(8,128)(2,1)} %param.21), kind=kOutput, calls=%fused_computation.1 | convolution fusion | flops 673710080 | bytes 10125312 | tf_op jit(solution)/shard_map/dot_general | solution.py:350
  185.7 4.0 %collective-permute-start.16 = (bf16[160,4096]{1,0:T(8,128)(2,1)S(1)}, bf16[160,4096]{1,0:T(8,128)(2,1)S(1)}, u32[]{:S(2)}, u32[]{:S(2)}) collective-permute-start(bf16[160,4096]{1,0:T(8,128)(2,1)S(1)} %slice.141), channel_id=1, source_target_pairs={{0,1},{1,0},{2,3},{3,2},{4,5},{5,4},{6,7},{7,6},{8,9},{9,8},{10,11... | collective-permute-start | bytes 3932168 | tf_op jit(solution)/shard_map/ppermute | solution.py:302
  189.7 2.6 %collective-permute-done.16 = bf16[160,4096]{1,0:T(8,128)(2,1)S(1)} collective-permute-done((bf16[160,4096]{1,0:T(8,128)(2,1)S(1)}, bf16[160,4096]{1,0:T(8,128)(2,1)S(1)}, u32[]{:S(2)}, u32[]{:S(2)}) %collective-permute-start.16) | collective-permute-done | bytes 1310752 | tf_op jit(solution)/shard_map/ppermute | solution.py:302
  192.7 20.1 %all_to_all.5 = bf16[4,40,4096]{2,1,0:T(8,128)(2,1)S(1)} all-to-all(bf16[4,40,4096]{2,1,0:T(8,128)(2,1)S(1)} %bitcast.57), channel_id=1, replica_groups=mesh['grp'=2,'hi'=8,'lo'=4,'x'=4,'core'=2] {'x'}, dimensions={0} | all-to-all | bytes 2621440 | tf_op jit(solution)/shard_map/all_to_all | solution.py:305
  (85 shorter events, 7.9 us)
Async XLA Ops:
  0.0 165.2 %copy-start = (bf16[256,4096]{1,0:T(8,128)(2,1)S(1)}, bf16[256,4096]{1,0:T(8,128)(2,1)}, u32[]{:S(2)}) copy-start(bf16[256,4096]{1,0:T(8,128)(2,1)} %param.20) | copy-start | bytes 6291460
  0.1 72.6 %copy-start.1 = (bf16[320,128]{1,0:T(8,128)(2,1)S(1)}, bf16[320,128]{1,0:T(8,128)(2,1)}, u32[]{:S(2)}) copy-start(bf16[320,128]{1,0:T(8,128)(2,1)} %param.12) | copy-start | bytes 245764
  0.1 72.6 %copy-start.2 = (bf16[320,128]{1,0:T(8,128)(2,1)S(1)}, bf16[320,128]{1,0:T(8,128)(2,1)}, u32[]{:S(2)}) copy-start(bf16[320,128]{1,0:T(8,128)(2,1)} %param.13) | copy-start | bytes 245764
  0.2 90.8 %copy-start.6 = (bf16[320,256]{1,0:T(8,128)(2,1)S(1)}, bf16[320,256]{1,0:T(8,128)(2,1)}, u32[]{:S(2)}) copy-start(bf16[320,256]{1,0:T(8,128)(2,1)} %param.11) | copy-start | bytes 491524
  7.0 93.4 %copy-start.7 = (bf16[640,128]{1,0:T(8,128)(2,1)}, bf16[640,128]{1,0:T(8,128)(2,1)S(1)}, u32[]{:S(2)}) copy-start(bf16[640,128]{1,0:T(8,128)(2,1)S(1)} %pad_maximum_fusion.2.refs_0_) | copy-start | bytes 491524
  7.0 84.1 %collective-permute-start.6 = (bf16[640,128]{1,0:T(8,128)(2,1)S(1)}, bf16[640,128]{1,0:T(8,128)(2,1)}, u32[]{:S(2)}, u32[]{:S(2)}) collective-permute-start(bf16[640,128]{1,0:T(8,128)(2,1)S(1)} %pad_maximum_fusion.2.refs_0_), channel_id=1, source_target_pairs={{0,24},{8,0},{16,8},{24,16},{1,25},{9,1},{17,9},{25,17},{2,26},{10... | collective-permute-start | bytes 491528 | tf_op jit(solution)/shard_map/ppermute | solution.py:211
  16.7 77.5 %collective-permute-start.5 = (bf16[640,128]{1,0:T(8,128)(2,1)S(1)}, bf16[640,128]{1,0:T(8,128)(2,1)}, u32[]{:S(2)}, u32[]{:S(2)}) collective-permute-start(bf16[640,128]{1,0:T(8,128)(2,1)S(1)} %pad_maximum_fusion.2.refs_0_), channel_id=1, source_target_pairs={{0,16},{8,24},{16,0},{24,8},{1,17},{9,25},{17,1},{25,9},{2,18},{10... | collective-permute-start | bytes 491528 | tf_op jit(solution)/shard_map/ppermute | solution.py:211
  18.6 81.7 %collective-permute-start.4 = (bf16[640,128]{1,0:T(8,128)(2,1)S(1)}, bf16[640,128]{1,0:T(8,128)(2,1)}, u32[]{:S(2)}, u32[]{:S(2)}) collective-permute-start(bf16[640,128]{1,0:T(8,128)(2,1)S(1)} %pad_maximum_fusion.2.refs_0_), channel_id=1, source_target_pairs={{0,8},{8,16},{16,24},{24,0},{1,9},{9,17},{17,25},{25,1},{2,10},{10... | collective-permute-start | bytes 491528 | tf_op jit(solution)/shard_map/ppermute | solution.py:211
  20.9 43.7 %collective-permute-start.1 = (bf16[320,256]{1,0:T(8,128)(2,1)}, bf16[320,256]{1,0:T(8,128)(2,1)}, u32[]{:S(2)}, u32[]{:S(2)}) collective-permute-start(bf16[320,256]{1,0:T(8,128)(2,1)} %shard_map.109.refs_4_), channel_id=1, source_target_pairs={{32,0},{64,32},{96,64},{128,96},{160,128},{192,160},{224,192},{0,2... | collective-permute-start | bytes 491528 | tf_op jit(solution)/shard_map/ppermute | solution.py:208
  62.0 10.7 %collective-permute-start = (bf16[320,256]{1,0:T(8,128)(2,1)}, bf16[320,256]{1,0:T(8,128)(2,1)}, u32[]{:S(2)}, u32[]{:S(2)}) collective-permute-start(bf16[320,256]{1,0:T(8,128)(2,1)} %shard_map.109.refs_4_), channel_id=1, source_target_pairs={{0,32},{32,64},{64,96},{96,128},{128,160},{160,192},{192,224},{224... | collective-permute-start | bytes 491528 | tf_op jit(solution)/shard_map/ppermute | solution.py:207
  73.3 33.3 %collective-permute-start.3 = (bf16[2,128,128]{2,1,0:T(8,128)(2,1)}, bf16[2,128,128]{2,1,0:T(8,128)(2,1)S(1)}, u32[]{:S(2)}, u32[]{:S(2)}) collective-permute-start(bf16[2,128,128]{2,1,0:T(8,128)(2,1)} %get-tuple-element.59), channel_id=1, source_target_pairs={{8,0},{16,8},{24,16},{32,24},{40,32},{48,40},{56,48},{64,56},{72,6... | collective-permute-start | bytes 196616 | tf_op jit(solution)/shard_map/ppermute | solution.py:250
  74.6 32.0 %collective-permute-start.2 = (bf16[2,128,128]{2,1,0:T(8,128)(2,1)}, bf16[2,128,128]{2,1,0:T(8,128)(2,1)S(1)}, u32[]{:S(2)}, u32[]{:S(2)}) collective-permute-start(bf16[2,128,128]{2,1,0:T(8,128)(2,1)} %get-tuple-element.60), channel_id=1, source_target_pairs={{0,8},{8,16},{16,24},{24,32},{32,40},{40,48},{48,56},{56,64},{64,7... | collective-permute-start | bytes 196616 | tf_op jit(solution)/shard_map/ppermute | solution.py:249
  91.1 18.0 %collective-permute-start.7 = (bf16[320,256]{1,0:T(8,128)(2,1)}, bf16[320,256]{1,0:T(8,128)(2,1)S(1)}, u32[]{:S(2)}, u32[]{:S(2)}) collective-permute-start(bf16[320,256]{1,0:T(8,128)(2,1)} %collective-permute-done.refs_5_), channel_id=1, source_target_pairs={{0,32},{32,64},{64,96},{96,128},{128,160},{160,192},{192,224},{224... | collective-permute-start | bytes 491528 | tf_op jit(solution)/shard_map/ppermute | solution.py:221
  94.2 17.7 %collective-permute-start.10 = (bf16[320,256]{1,0:T(8,128)(2,1)}, bf16[320,256]{1,0:T(8,128)(2,1)}, u32[]{:S(2)}, u32[]{:S(2)}) collective-permute-start(bf16[320,256]{1,0:T(8,128)(2,1)} %collective-permute-done.1.refs_6_), channel_id=1, source_target_pairs={{32,0},{64,32},{96,64},{128,96},{160,128},{192,160},{224,192},{0,2... | collective-permute-start | bytes 491528 | tf_op jit(solution)/shard_map/ppermute | solution.py:221
  106.7 0.7 copy-start.12
  109.1 28.4 %copy-start.13 = (bf16[320,256]{1,0:T(8,128)(2,1)}, bf16[320,256]{1,0:T(8,128)(2,1)S(1)}, u32[]{:S(2)}) copy-start(bf16[320,256]{1,0:T(8,128)(2,1)S(1)} %collective-permute-done.7.refs_1_) | copy-start | bytes 491524
  109.1 18.9 %collective-permute-start.8 = (bf16[320,256]{1,0:T(8,128)(2,1)S(1)}, bf16[320,256]{1,0:T(8,128)(2,1)S(1)}, u32[]{:S(2)}, u32[]{:S(2)}) collective-permute-start(bf16[320,256]{1,0:T(8,128)(2,1)S(1)} %collective-permute-done.7.refs_1_), channel_id=1, source_target_pairs={{0,32},{32,64},{64,96},{96,128},{128,160},{160,192},{192,224},{224... | collective-permute-start | bytes 491528 | tf_op jit(solution)/shard_map/ppermute | solution.py:221
  111.8 18.1 %collective-permute-start.11 = (bf16[320,256]{1,0:T(8,128)(2,1)}, bf16[320,256]{1,0:T(8,128)(2,1)S(1)}, u32[]{:S(2)}, u32[]{:S(2)}) collective-permute-start(bf16[320,256]{1,0:T(8,128)(2,1)} %collective-permute-done.10.refs_2_), channel_id=1, source_target_pairs={{32,0},{64,32},{96,64},{128,96},{160,128},{192,160},{224,192},{0,2... | collective-permute-start | bytes 491528 | tf_op jit(solution)/shard_map/ppermute | solution.py:221
  128.0 15.1 %copy-start.10 = (bf16[320,256]{1,0:T(8,128)(2,1)}, bf16[320,256]{1,0:T(8,128)(2,1)S(1)}, u32[]{:S(2)}) copy-start(bf16[320,256]{1,0:T(8,128)(2,1)S(1)} %collective-permute-done.8.refs_1_) | copy-start | bytes 491524
  128.0 20.7 %collective-permute-start.9 = (bf16[320,128]{1,0:T(8,128)(2,1)S(1)}, bf16[320,128]{1,0:T(8,128)(2,1)S(1)}, u32[]{:S(2)}, u32[]{:S(2)}) collective-permute-start(bf16[320,128]{1,0:T(8,128)(2,1)S(1)} %slice.138), channel_id=1, source_target_pairs={{0,32},{32,64},{64,96},{96,128},{128,160},{160,192},{192,224},{224... | collective-permute-start | bytes 245768 | tf_op jit(solution)/shard_map/ppermute | solution.py:221
  130.0 13.1 %copy-start.11 = (bf16[320,256]{1,0:T(8,128)(2,1)}, bf16[320,256]{1,0:T(8,128)(2,1)S(1)}, u32[]{:S(2)}) copy-start(bf16[320,256]{1,0:T(8,128)(2,1)S(1)} %collective-permute-done.11.refs_2_) | copy-start | bytes 491524
  130.0 18.7 %collective-permute-start.12 = (bf16[320,128]{1,0:T(8,128)(2,1)S(1)}, bf16[320,128]{1,0:T(8,128)(2,1)S(1)}, u32[]{:S(2)}, u32[]{:S(2)}) collective-permute-start(bf16[320,128]{1,0:T(8,128)(2,1)S(1)} %slice.139), channel_id=1, source_target_pairs={{32,0},{64,32},{96,64},{128,96},{160,128},{192,160},{224,192},{0,2... | collective-permute-start | bytes 245768 | tf_op jit(solution)/shard_map/ppermute | solution.py:221
  148.7 0.6 copy-start.8
  148.7 0.7 copy-start.9
  153.5 15.0 %collective-permute-start.13 = (bf16[160,640]{1,0:T(8,128)(2,1)}, bf16[160,640]{1,0:T(8,128)(2,1)S(1)}, u32[]{:S(2)}, u32[]{:S(2)}) collective-permute-start(bf16[160,640]{1,0:T(8,128)(2,1)} %get-tuple-element.42), channel_id=1, source_target_pairs={{0,24},{8,0},{16,8},{24,16},{1,25},{9,1},{17,9},{25,17},{2,26},{10... | collective-permute-start | bytes 614408 | tf_op jit(solution)/shard_map/ppermute | solution.py:230
  159.5 19.2 %collective-permute-start.14 = (bf16[160,640]{1,0:T(8,128)(2,1)}, bf16[160,640]{1,0:T(8,128)(2,1)S(1)}, u32[]{:S(2)}, u32[]{:S(2)}) collective-permute-start(bf16[160,640]{1,0:T(8,128)(2,1)} %get-tuple-element.43), channel_id=1, source_target_pairs={{0,16},{8,24},{16,0},{24,8},{1,17},{9,25},{17,1},{25,9},{2,18},{10... | collective-permute-start | bytes 614408 | tf_op jit(solution)/shard_map/ppermute | solution.py:230
  163.3 15.4 %collective-permute-start.15 = (bf16[160,640]{1,0:T(8,128)(2,1)}, bf16[160,640]{1,0:T(8,128)(2,1)S(1)}, u32[]{:S(2)}, u32[]{:S(2)}) collective-permute-start(bf16[160,640]{1,0:T(8,128)(2,1)} %get-tuple-element.44), channel_id=1, source_target_pairs={{0,8},{8,16},{16,24},{24,0},{1,9},{9,17},{17,25},{25,1},{2,10},{10... | collective-permute-start | bytes 614408 | tf_op jit(solution)/shard_map/ppermute | solution.py:230
  168.4 10.3 %copy-start.3 = (bf16[160,640]{1,0:T(8,128)(2,1)}, bf16[160,640]{1,0:T(8,128)(2,1)S(1)}, u32[]{:S(2)}) copy-start(bf16[160,640]{1,0:T(8,128)(2,1)S(1)} %collective-permute-done.13.refs_1_) | copy-start | bytes 614404
  178.7 0.7 copy-start.4
  178.7 0.8 copy-start.5
  185.7 6.6 %collective-permute-start.16 = (bf16[160,4096]{1,0:T(8,128)(2,1)S(1)}, bf16[160,4096]{1,0:T(8,128)(2,1)S(1)}, u32[]{:S(2)}, u32[]{:S(2)}) collective-permute-start(bf16[160,4096]{1,0:T(8,128)(2,1)S(1)} %slice.141), channel_id=1, source_target_pairs={{0,1},{1,0},{2,3},{3,2},{4,5},{5,4},{6,7},{7,6},{8,9},{9,8},{10,11... | collective-permute-start | bytes 3932168 | tf_op jit(solution)/shard_map/ppermute | solution.py:302
where the time goes:
time: 215 us; the launch traced here: 214 us
  starting transfers between devices  118 us (55%)
  waiting for transfers between devices  31 us (14%)
  Pallas kernels  27.9 us (13%)
  blocking collectives  20.1 us (9%)
  matrix products  8.07 us (4%)
  other arithmetic  5.87 us (3%)
  local copies, waits for them, and re-layouts  2.17 us (1%)
    ppermute x1, starting transfers between devices, grid_attend(): behind = lax.ppermute(kv, 'hi', back)  41.1 us
    pallas_call x4, Pallas kernels, attend(): pl.pallas_call(functools.partial(attend_kernel, planes=len(queries), piec...  21.5 us
    ppermute x3, starting transfers between devices, grid_attend(): lax.ppermute(next_behind, 'hi', back)  20.1 us
    all_to_all x1, blocking collectives, sent_and_summed(): tiles = lax.all_to_all(tiles, 'x', 0, 0, tiled=True)  20.1 us
    ppermute x1, starting transfers between devices, extended(): above = lax.ppermute(tail, axes, [(i, i + 1) for i in range(ends)])  16.3 us
    ppermute x3, starting transfers between devices, grid_attend(): lax.ppermute(queries, 'lo', [(i, (i + d) % low) for i in range(low)])  13.9 us
    ppermute x3, starting transfers between devices, grid_attend(): lax.ppermute(parts[d], 'lo', [(i, (i - d) % low) for i in range(low)])  11.8 us
    ppermute x3, waiting for transfers between devices, grid_attend(): lax.ppermute(parts[d], 'lo', [(i, (i - d) % low) for i in range(low)])  10.3 us
  transfers between devices with their start and end apart: 17, of which 5 were waited for; matrix products, arithmetic and copies ran while one was open for 3% of the time, Pallas kernels for 8%

commit v1 on v0

--- a/solution.py
+++ b/solution.py
@@ -18,7 +18,7 @@
 EPSILON = 1e-06
 CORES = 2
 PLANES = 4
-TAIL = 32
+TAIL = 16
 
 
 def turn_tables(offset, local_rows):
@@ -121,12 +121,10 @@
         left = weight - high.astype(jnp.float32)
         middle = left.astype(jnp.bfloat16)
         low = (left - middle.astype(jnp.float32)).astype(jnp.bfloat16)
-        terms = [high, middle, low]
-        tail = jnp.concatenate(
-            [jnp.broadcast_to(t.astype(jnp.float32), (8, chunk)) for t in terms]
-            + [jnp.zeros((8, chunk), jnp.float32)],
-            axis=0,
-        )
+        line = lax.broadcasted_iota(jnp.int32, (TAIL, chunk), 0)
+        tail = jnp.zeros((TAIL, chunk), jnp.float32)
+        for row, term in enumerate((high, middle, low)):
+            tail = jnp.where(line == row, term.astype(jnp.float32), tail)
         out = (acc / total).astype(jnp.bfloat16)
         tail = tail.astype(jnp.bfloat16)
         each = rows // len(rest)
@@ -176,29 +174,62 @@
     )(*queries, *kvs, *(carry or ()))
 
 
-def merge_kernel(*refs):
-    o_ref = refs[-1]
-    heads = o_ref.shape[1] // HEAD
-    count = o_ref.shape[0]
-    parts = refs[:-1]
-    weights = [
-        r[HEAD : HEAD + 8, :].astype(jnp.float32)[:1]
-        + r[HEAD + 8 : HEAD + 16, :].astype(jnp.float32)[:1]
-        + r[HEAD + 16 : HEAD + 24, :].astype(jnp.float32)[:1]
-        for r in parts
-    ]
-    top = functools.reduce(jnp.maximum, weights)
-    shares = [jnp.exp2(w - top) for w in weights]
-    total = functools.reduce(jnp.add, shares)
-    out = functools.reduce(
-        jnp.add, [r[:HEAD, :].astype(jnp.float32) * s for r, s in zip(parts, shares)]
-    )
-    out = (out / total).T.astype(jnp.bfloat16)
-    for h in range(heads):
-        o_ref[:, h * HEAD : (h + 1) * HEAD] = out[h * count : (h + 1) * count, :]
-
-
-def grid_attend(kv, make_queries, heads, held):
+def project_kernel(*refs, count):
+    parts = refs[:count]
+    window_ref, window_weights_ref, grid_weights_ref, here_ref, there_ref, grid_ref = refs[count:]
+
+    @pl.when(pl.program_id(0) == 0)
+    def _():
+        rows = grid_ref.shape[0]
+        weights = [
+            jnp.sum(r[HEAD:, :].astype(jnp.float32), axis=0, keepdims=True) for r in parts
+        ]
+        top = functools.reduce(jnp.maximum, weights)
+        shares = [jnp.exp2(w - top) for w in weights]
+        total = functools.reduce(jnp.add, shares)
+        out = functools.reduce(
+            jnp.add, [r[:HEAD, :].astype(jnp.float32) * s for r, s in zip(parts, shares)]
+        )
+        out = (out / total).T.astype(jnp.bfloat16)
+        for h in range(grid_ref.shape[1] // HEAD):
+            grid_ref[:, h * HEAD : (h + 1) * HEAD] = out[h * rows : (h + 1) * rows, :]
+
+    partial = jnp.dot(
+        window_ref[...], window_weights_ref[...], preferred_element_type=jnp.float32
+    ) + jnp.dot(grid_ref[...], grid_weights_ref[...], preferred_element_type=jnp.float32)
+    half = here_ref.shape[0]
+    here_ref[...] = partial[:half].astype(jnp.bfloat16)
+    there_ref[...] = partial[half:].astype(jnp.bfloat16)
+
+
+def project(parts, window_out, window_weights, grid_weights, columns=1024):
+    rows, width = window_out.shape
+    total = window_weights.shape[1]
+    grid_width = grid_weights.shape[0]
+    half = jax.ShapeDtypeStruct((rows // CORES, total), jnp.bfloat16)
+    whole = lambda a: pl.BlockSpec(a.shape, lambda j: (0, 0))
+    return pl.pallas_call(
+        functools.partial(project_kernel, count=len(parts)),
+        grid=(total // columns,),
+        in_specs=[whole(p) for p in parts]
+        + [
+            whole(window_out),
+            pl.BlockSpec((width, columns), lambda j: (0, j)),
+            pl.BlockSpec((grid_width, columns), lambda j: (0, j)),
+        ],
+        out_specs=[pl.BlockSpec((rows // CORES, columns), lambda j: (0, j))] * CORES,
+        out_shape=(half,) * CORES,
+        scratch_shapes=[pltpu.VMEM((rows, grid_width), jnp.bfloat16)],
+        compiler_params=pltpu.CompilerParams(dimension_semantics=("arbitrary",)),
+        cost_estimate=pl.CostEstimate(
+            flops=2 * rows * (width + grid_width) * total,
+            bytes_accessed=2 * total * (width + grid_width + rows),
+            transcendentals=rows,
+        ),
+    )(*parts, window_out, window_weights, grid_weights)
+
+
+def grid_attend(kv, make_queries, held):
     high = lax.axis_size("hi")
     low = lax.axis_size("lo")
     ring = [(i, (i + 1) % high) for i in range(high)]
@@ -211,7 +242,7 @@
         lax.ppermute(queries, "lo", [(i, (i + d) % low) for i in range(low)])
         for d in range(1, low)
     ]
-    ahead, behind, held = lax.optimization_barrier((ahead, behind, held))
+    ahead, behind, held, shared[0] = lax.optimization_barrier((ahead, behind, held, shared[0]))
     rows, carry, waiting = shared, None, (kv,)
     for step in range(1, high // 2):
         if step + 1 < high // 2:
@@ -230,15 +261,7 @@
         lax.ppermute(parts[d], "lo", [(i, (i - d) % low) for i in range(low)])
         for d in range(1, low)
     ]
-    count = parts[0].shape[1]
-    grid_out = pl.pallas_call(
-        merge_kernel,
-        out_shape=jax.ShapeDtypeStruct((count // heads, heads * HEAD), jnp.bfloat16),
-        cost_estimate=pl.CostEstimate(
-            flops=8 * count * HEAD, bytes_accessed=count * HEAD * 10, transcendentals=count
-        ),
-    )(*parts)
-    return grid_out, held
+    return parts, held
 
 
 def extended(cells, axes, width):
@@ -289,21 +312,26 @@
 
 def by_target(rows):
     across = lax.axis_size("x")
+    x = lax.axis_index("x")
     core = lax.axis_index("core")
     count = rows.shape[0] // (across * CORES)
     tiles = rows.reshape(across, CORES, count, rows.shape[1])
     tiles = jnp.where(core == 0, tiles, tiles[:, ::-1])
+    tiles = lax.dynamic_slice_in_dim(jnp.concatenate([tiles, tiles], axis=0), x, across, axis=0)
     return jnp.swapaxes(tiles, 0, 1).reshape(rows.shape)
 
 
-def sent_and_summed(partial):
-    half = partial.shape[0] // CORES
+def sent_and_summed(here, there):
     across = lax.axis_size("x")
-    theirs = lax.ppermute(partial[half:], "core", [(0, 1), (1, 0)])
-    both = partial[:half].astype(jnp.float32) + theirs.astype(jnp.float32)
-    tiles = both.astype(jnp.bfloat16).reshape(across, half // across, -1)
-    tiles = lax.all_to_all(tiles, "x", 0, 0, tiled=True)
-    return jnp.sum(tiles.astype(jnp.float32), axis=0)
+    theirs = lax.ppermute(there, "core", [(0, 1), (1, 0)])
+    both = here.astype(jnp.float32) + theirs.astype(jnp.float32)
+    tiles = both.astype(jnp.bfloat16).reshape(across, here.shape[0] // across, -1)
+    total = tiles[0].astype(jnp.float32)
+    for d in range(1, across):
+        total = total + lax.ppermute(
+            tiles[d], "x", [(i, (i + d) % across) for i in range(across)]
+        ).astype(jnp.float32)
+    return total
 
 
 def per_device(
@@ -336,8 +364,8 @@
             [turned[:, h * HEAD : (h + 1) * HEAD] for h in range(heads)], axis=0
         )
 
-    grid_out, (window_query, window_key, window_value) = grid_attend(
-        kv, make_queries, heads, (window_query, window_key, window_value)
+    parts, (window_query, window_key, window_value) = grid_attend(
+        kv, make_queries, (window_query, window_key, window_value)
     )
 
     local_heads = sink_logit.shape[0]
@@ -347,10 +375,8 @@
     window_out = by_target(
         window_attend(window_query, padded[0], padded[1], slopes, sink_logit, offset, total_rows)
     )
-    partial = jnp.dot(window_out, window_weights, preferred_element_type=jnp.float32) + jnp.dot(
-        grid_out, grid_weights, preferred_element_type=jnp.float32
-    )
-    return sent_and_summed(partial.astype(jnp.bfloat16)).astype(jnp.bfloat16)
+    here, there = project(parts, window_out, window_weights, grid_weights)
+    return sent_and_summed(here, there).astype(jnp.bfloat16)
 
 
 def solution(mesh):

time: 215 us -> 200 us (0.930)
  blocking collectives: 20.1 us -> 0 us
  starting transfers between devices: 118 us -> 129 us
  matrix products: 8.07 us -> 0.85 us
  waiting for transfers between devices: 31 us -> 27.3 us
  Pallas kernels: 27.9 us -> 31.4 us
    all_to_all x1 -> x0, blocking collectives: 20.1 us -> none  [sent_and_summed(): tiles = lax.all_to_all(tiles, 'x', 0, 0, tiled=True)]
    ppermute x1, starting transfers between devices: 16.3 us -> 2.64 us  [extended(): above = lax.ppermute(tail, axes, [(i, i + 1) for i in range(ends)])]
    ppermute x1 -> x4, waiting for transfers between devices: 2.64 us -> 14.5 us  [the longest x3 11.7 us: sent_and_summed(): lax.ppermute(tiles[d], 'x', [(i, (i + d) % across) for i in range(across)])]
    ppermute x1, starting transfers between devices: 1.95 us -> 13.1 us  [grid_attend(): ahead = lax.ppermute(kv, 'hi', ring)]
    ppermute x3, waiting for transfers between devices: 9.95 us -> 0.01 us  [grid_attend(): lax.ppermute(next_ahead, 'hi', ring)]
    ppermute x1 -> x4, starting transfers between devices: 3.95 us -> 13.9 us  [the longest x3 9.66 us: sent_and_summed(): lax.ppermute(tiles[d], 'x', [(i, (i + d) % across) for i in range(across)])]
    ppermute x1, waiting for transfers between devices: 8.13 us -> 0.01 us  [grid_attend(): ahead = lax.ppermute(kv, 'hi', ring)]
    ppermute x3, starting transfers between devices: 11.8 us -> 19.4 us  [grid_attend(): lax.ppermute(parts[d], 'lo', [(i, (i - d) % low) for i in range(low)])]
  transfers between devices with their start and end apart: 17 -> 20, of which waited for: 5 -> 6; matrix products, arithmetic and copies ran while one was open for 3% -> 2% of each run, Pallas kernels for 8% -> 10%
where the time goes in v1:
time: 200 us; the launch traced here: 199 us
  starting transfers between devices  129 us (64%)
  Pallas kernels  31.4 us (16%)
  waiting for transfers between devices  27.3 us (14%)
  other arithmetic  6.62 us (3%)
  local copies, waits for them, and re-layouts  3.54 us (2%)
    ppermute x1, starting transfers between devices, grid_attend(): behind = lax.ppermute(kv, 'hi', back)  33.5 us
    ppermute x3, starting transfers between devices, grid_attend(): lax.ppermute(next_behind, 'hi', back)  24.8 us
    pallas_call x4, Pallas kernels, attend(): pl.pallas_call(functools.partial(attend_kernel, planes=len(queries), piec...  21.6 us
    ppermute x3, starting transfers between devices, grid_attend(): lax.ppermute(parts[d], 'lo', [(i, (i - d) % low) for i in range(low)])  19.4 us
    ppermute x1, starting transfers between devices, grid_attend(): ahead = lax.ppermute(kv, 'hi', ring)  13.1 us
    ppermute x3, waiting for transfers between devices, sent_and_summed(): lax.ppermute(tiles[d], 'x', [(i, (i + d) % across) for i in range(across)])  11.7 us
    ppermute x3, starting transfers between devices, grid_attend(): lax.ppermute(queries, 'lo', [(i, (i + d) % low) for i in range(low)])  11.1 us
    ppermute x3, waiting for transfers between devices, grid_attend(): lax.ppermute(parts[d], 'lo', [(i, (i - d) % low) for i in range(low)])  10.6 us
  transfers between devices with their start and end apart: 20, of which 6 were waited for; matrix products, arithmetic and copies ran while one was open for 2% of the time, Pallas kernels for 10%

profile of v1, /device:TPU:33, one launch (start us, length us, event | category | flops | bytes accessed | tf_op | source)
XLA Modules:
  0.0 199.1 jit_solution(7151049884316656216)
XLA Ops:
  1.6 2.0 %shard_map.109.refs_4_ = bf16[320,256]{1,0:T(8,128)(2,1)} custom-call(bf16[320,128]{1,0:T(8,128)(2,1)} %x_ref.1, f32[1,128]{1,0:T(1,128)} %bitcast.69, f32[320,128]{1,0:T(8,128)} %get-tuple-element.55.cos_ref, f32[320,128]{1,0:T(8,128)} %get-tuple-element.54.sin_ref, bf16[320,128]{1,0:T(8,128)(2,1)} %rest_0_.1), custom_call_target="tpu_custom_call" | custom-call | flops 1310720 | bytes 655360 | tf_op jit(solution)/shard_map/pallas_call | solution.py:59
  3.6 13.1 %collective-permute-start = (bf16[320,256]{1,0:T(8,128)(2,1)}, bf16[320,256]{1,0:T(8,128)(2,1)S(1)}, u32[]{:S(2)}, u32[]{:S(2)}) collective-permute-start(bf16[320,256]{1,0:T(8,128)(2,1)} %shard_map.109.refs_4_), channel_id=1, source_target_pairs={{0,32},{32,64},{64,96},{96,128},{128,160},{160,192},{192,224},{224... | collective-permute-start | bytes 491528 | tf_op jit(solution)/shard_map/ppermute | solution.py:238
  16.7 33.5 %collective-permute-start.1 = (bf16[320,256]{1,0:T(8,128)(2,1)}, bf16[320,256]{1,0:T(8,128)(2,1)S(1)}, u32[]{:S(2)}, u32[]{:S(2)}) collective-permute-start(bf16[320,256]{1,0:T(8,128)(2,1)} %shard_map.109.refs_4_), channel_id=1, source_target_pairs={{32,0},{64,32},{96,64},{128,96},{160,128},{192,160},{224,192},{0,2... | collective-permute-start | bytes 491528 | tf_op jit(solution)/shard_map/ppermute | solution.py:239
  50.2 2.2 %shard_map.110 = bf16[320,256]{1,0:T(8,128)(2,1)} custom-call(bf16[320,256]{1,0:T(8,128)(2,1)} %x_ref.2, f32[1,128]{1,0:T(1,128)} %bitcast.70, f32[320,128]{1,0:T(8,128)} %get-tuple-element.55.cos_ref, f32[320,128]{1,0:T(8,128)} %get-tuple-element.54.sin_ref), custom_call_target="tpu_custom_call" | custom-call | flops 1310720 | bytes 655360 | tf_op jit(solution)/shard_map/pallas_call | solution.py:59
  53.7 3.5 %collective-permute-start.2 = (bf16[640,128]{1,0:T(8,128)(2,1)S(1)}, bf16[640,128]{1,0:T(8,128)(2,1)S(1)}, u32[]{:S(2)}, u32[]{:S(2)}) collective-permute-start(bf16[640,128]{1,0:T(8,128)(2,1)S(1)} %pad_maximum_fusion.2.refs_0_), channel_id=1, source_target_pairs={{0,8},{8,16},{16,24},{24,0},{1,9},{9,17},{17,25},{25,1},{2,10},{10... | collective-permute-start | bytes 491528 | tf_op jit(solution)/shard_map/ppermute | solution.py:242
  57.2 4.8 %collective-permute-start.3 = (bf16[640,128]{1,0:T(8,128)(2,1)S(1)}, bf16[640,128]{1,0:T(8,128)(2,1)S(1)}, u32[]{:S(2)}, u32[]{:S(2)}) collective-permute-start(bf16[640,128]{1,0:T(8,128)(2,1)S(1)} %pad_maximum_fusion.2.refs_0_), channel_id=1, source_target_pairs={{0,16},{8,24},{16,0},{24,8},{1,17},{9,25},{17,1},{25,9},{2,18},{10... | collective-permute-start | bytes 491528 | tf_op jit(solution)/shard_map/ppermute | solution.py:242
  62.1 2.7 %collective-permute-start.4 = (bf16[640,128]{1,0:T(8,128)(2,1)S(1)}, bf16[640,128]{1,0:T(8,128)(2,1)S(1)}, u32[]{:S(2)}, u32[]{:S(2)}) collective-permute-start(bf16[640,128]{1,0:T(8,128)(2,1)S(1)} %pad_maximum_fusion.2.refs_0_), channel_id=1, source_target_pairs={{0,24},{8,0},{16,8},{24,16},{1,25},{9,1},{17,9},{25,17},{2,26},{10... | collective-permute-start | bytes 491528 | tf_op jit(solution)/shard_map/ppermute | solution.py:242
  65.5 2.6 %collective-permute-start.14 = (bf16[2,128,128]{2,1,0:T(8,128)(2,1)S(1)}, bf16[2,128,128]{2,1,0:T(8,128)(2,1)S(1)}, u32[]{:S(2)}, u32[]{:S(2)}) collective-permute-start(bf16[2,128,128]{2,1,0:T(8,128)(2,1)S(1)} %get-tuple-element.67), channel_id=1, source_target_pairs={{0,8},{8,16},{16,24},{24,32},{32,40},{40,48},{48,56},{56,64},{64,7... | collective-permute-start | bytes 196616 | tf_op jit(solution)/shard_map/ppermute | solution.py:272
  69.5 4.9 %collective-permute-start.5 = (bf16[320,256]{1,0:T(8,128)(2,1)S(1)}, bf16[320,256]{1,0:T(8,128)(2,1)S(1)}, u32[]{:S(2)}, u32[]{:S(2)}) collective-permute-start(bf16[320,256]{1,0:T(8,128)(2,1)S(1)} %collective-permute-done.refs_5_), channel_id=1, source_target_pairs={{0,32},{32,64},{64,96},{96,128},{128,160},{160,192},{192,224},{224... | collective-permute-start | bytes 491528 | tf_op jit(solution)/shard_map/ppermute | solution.py:252
  74.4 8.2 %collective-permute-start.8 = (bf16[320,256]{1,0:T(8,128)(2,1)S(1)}, bf16[320,256]{1,0:T(8,128)(2,1)S(1)}, u32[]{:S(2)}, u32[]{:S(2)}) collective-permute-start(bf16[320,256]{1,0:T(8,128)(2,1)S(1)} %collective-permute-done.1.refs_6_), channel_id=1, source_target_pairs={{32,0},{64,32},{96,64},{128,96},{160,128},{192,160},{224,192},{0,2... | collective-permute-start | bytes 491528 | tf_op jit(solution)/shard_map/ppermute | solution.py:252
  83.3 6.3 %shard_map.111 = (f32[1,2560]{1,0:T(1,128)}, f32[1,2560]{1,0:T(1,128)}, f32[128,2560]{1,0:T(8,128)}, bf16[2560,128]{1,0:T(8,128)(2,1)}) custom-call(bf16[640,128]{1,0:T(8,128)(2,1)} %copy-done.6, bf16[640,128]{1,0:T(8,128)(2,1)} %copy-done.16, bf16[640,128]{1,0:T(8,128)(2,1)} %copy-done.17, bf16[640,128]{1,0:T(8,128)(2,1)} %copy-done.18, ...), custom_call_target="tpu_custom_call" | custom-call | flops 1258291200 | bytes 3276800 | tf_op jit(solution)/shard_map/pallas_call | solution.py:164
  91.1 2.0 collective-permute-start.6
  93.1 7.3 %collective-permute-start.9 = (bf16[320,256]{1,0:T(8,128)(2,1)S(1)}, bf16[320,256]{1,0:T(8,128)(2,1)S(1)}, u32[]{:S(2)}, u32[]{:S(2)}) collective-permute-start(bf16[320,256]{1,0:T(8,128)(2,1)S(1)} %collective-permute-done.8.refs_2_), channel_id=1, source_target_pairs={{32,0},{64,32},{96,64},{128,96},{160,128},{192,160},{224,192},{0,2... | collective-permute-start | bytes 491528 | tf_op jit(solution)/shard_map/ppermute | solution.py:252
  101.1 2.1 %collective-permute-done.9.refs_2_ = bf16[320,256]{1,0:T(8,128)(2,1)S(1)} collective-permute-done((bf16[320,256]{1,0:T(8,128)(2,1)S(1)}, bf16[320,256]{1,0:T(8,128)(2,1)S(1)}, u32[]{:S(2)}, u32[]{:S(2)}) %collective-permute-start.9) | collective-permute-done | bytes 163872 | tf_op jit(solution)/shard_map/ppermute | solution.py:252
  103.2 9.3 %collective-permute-start.10 = (bf16[320,128]{1,0:T(8,128)(2,1)S(1)}, bf16[320,128]{1,0:T(8,128)(2,1)S(1)}, u32[]{:S(2)}, u32[]{:S(2)}) collective-permute-start(bf16[320,128]{1,0:T(8,128)(2,1)S(1)} %slice.143), channel_id=1, source_target_pairs={{32,0},{64,32},{96,64},{128,96},{160,128},{192,160},{224,192},{0,2... | collective-permute-start | bytes 245768 | tf_op jit(solution)/shard_map/ppermute | solution.py:252
  112.6 2.1 %collective-permute-start.7 = (bf16[320,128]{1,0:T(8,128)(2,1)S(1)}, bf16[320,128]{1,0:T(8,128)(2,1)S(1)}, u32[]{:S(2)}, u32[]{:S(2)}) collective-permute-start(bf16[320,128]{1,0:T(8,128)(2,1)S(1)} %slice.142), channel_id=1, source_target_pairs={{0,32},{32,64},{64,96},{96,128},{128,160},{160,192},{192,224},{224... | collective-permute-start | bytes 245768 | tf_op jit(solution)/shard_map/ppermute | solution.py:252
  114.7 5.6 %shard_map.112 = (f32[1,2560]{1,0:T(1,128)}, f32[1,2560]{1,0:T(1,128)}, f32[128,2560]{1,0:T(8,128)}) custom-call(bf16[2560,128]{1,0:T(8,128)(2,1)} %get-tuple-element.32.refs_0_, bf16[320,256]{1,0:T(8,128)(2,1)} %copy-done.14, bf16[320,256]{1,0:T(8,128)(2,1)} %copy-done.15, f32[1,2560]{1,0:T(1,128)} %get-tuple-element.33.refs_3_, ...), custom_call_target="tpu_custom_call" | custom-call | flops 838860800 | bytes 3276800 | tf_op jit(solution)/shard_map/pallas_call | solution.py:164
  120.3 5.6 %shard_map.113 = (f32[1,2560]{1,0:T(1,128)}, f32[1,2560]{1,0:T(1,128)}, f32[128,2560]{1,0:T(8,128)}) custom-call(bf16[2560,128]{1,0:T(8,128)(2,1)} %get-tuple-element.32.refs_0_, bf16[320,256]{1,0:T(8,128)(2,1)} %copy-done.9, bf16[320,256]{1,0:T(8,128)(2,1)} %copy-done.10, f32[1,2560]{1,0:T(1,128)} %get-tuple-element.36.refs_3_, ...), custom_call_target="tpu_custom_call" | custom-call | flops 838860800 | bytes 3276800 | tf_op jit(solution)/shard_map/pallas_call | solution.py:164
  126.6 4.1 %shard_map.114 = (bf16[144,640]{1,0:T(8,128)(2,1)}, bf16[144,640]{1,0:T(8,128)(2,1)}, bf16[144,640]{1,0:T(8,128)(2,1)}, bf16[144,640]{1,0:T(8,128)(2,1)}) custom-call(bf16[2560,128]{1,0:T(8,128)(2,1)} %get-tuple-element.32.refs_0_, bf16[320,128]{1,0:T(8,128)(2,1)} %copy-done.8, bf16[320,128]{1,0:T(8,128)(2,1)} %copy-done.7, ...), custom_call_target="tpu_custom_call" | custom-call | flops 419430400 | bytes 3276800 | tf_op jit(solution)/shard_map/pallas_call | solution.py:164
  130.7 12.1 %collective-permute-start.11 = (bf16[144,640]{1,0:T(8,128)(2,1)}, bf16[144,640]{1,0:T(8,128)(2,1)S(1)}, u32[]{:S(2)}, u32[]{:S(2)}) collective-permute-start(bf16[144,640]{1,0:T(8,128)(2,1)} %get-tuple-element.43), channel_id=1, source_target_pairs={{0,24},{8,0},{16,8},{24,16},{1,25},{9,1},{17,9},{25,17},{2,26},{10... | collective-permute-start | bytes 552968 | tf_op jit(solution)/shard_map/ppermute | solution.py:261
  142.7 5.4 %collective-permute-start.12 = (bf16[144,640]{1,0:T(8,128)(2,1)}, bf16[144,640]{1,0:T(8,128)(2,1)S(1)}, u32[]{:S(2)}, u32[]{:S(2)}) collective-permute-start(bf16[144,640]{1,0:T(8,128)(2,1)} %get-tuple-element.44), channel_id=1, source_target_pairs={{0,16},{8,24},{16,0},{24,8},{1,17},{9,25},{17,1},{25,9},{2,18},{10... | collective-permute-start | bytes 552968 | tf_op jit(solution)/shard_map/ppermute | solution.py:261
  148.2 2.0 collective-permute-start.13
  151.0 10.6 %collective-permute-done.12.refs_2_ = bf16[144,640]{1,0:T(8,128)(2,1)S(1)} collective-permute-done((bf16[144,640]{1,0:T(8,128)(2,1)}, bf16[144,640]{1,0:T(8,128)(2,1)S(1)}, u32[]{:S(2)}, u32[]{:S(2)}) %collective-permute-start.12) | collective-permute-done | bytes 184352 | tf_op jit(solution)/shard_map/ppermute | solution.py:261
  162.3 5.7 %shard_map.115 = (bf16[160,4096]{1,0:T(8,128)(2,1)}, bf16[160,4096]{1,0:T(8,128)(2,1)}) custom-call(bf16[144,640]{1,0:T(8,128)(2,1)} %get-tuple-element.42.refs_0_, bf16[144,640]{1,0:T(8,128)(2,1)} %copy-done.2, bf16[144,640]{1,0:T(8,128)(2,1)} %copy-done.3, bf16[144,640]{1,0:T(8,128)(2,1)} %copy-done.4, bf16[320,256]{1,0:T(8,128)(2,1)} %bitcast.58, ...), custom_call_target="tpu_custom_call" | custom-call | flops 1342177280 | bytes 6815744 | tf_op jit(solution)/shard_map/pallas_call | solution.py:211
  168.0 4.2 %collective-permute-start.16 = (bf16[160,4096]{1,0:T(8,128)(2,1)}, bf16[160,4096]{1,0:T(8,128)(2,1)S(1)}, u32[]{:S(2)}, u32[]{:S(2)}) collective-permute-start(bf16[160,4096]{1,0:T(8,128)(2,1)} %get-tuple-element.50), channel_id=1, source_target_pairs={{0,1},{1,0},{2,3},{3,2},{4,5},{5,4},{6,7},{7,6},{8,9},{9,8},{10,11... | collective-permute-start | bytes 3932168 | tf_op jit(solution)/shard_map/ppermute | solution.py:326
  172.2 2.9 %collective-permute-done.16 = bf16[160,4096]{1,0:T(8,128)(2,1)S(1)} collective-permute-done((bf16[160,4096]{1,0:T(8,128)(2,1)}, bf16[160,4096]{1,0:T(8,128)(2,1)S(1)}, u32[]{:S(2)}, u32[]{:S(2)}) %collective-permute-start.16) | collective-permute-done | bytes 1310752 | tf_op jit(solution)/shard_map/ppermute | solution.py:326
  176.8 2.0 %collective-permute-start.17 = (bf16[40,4096]{1,0:T(8,128)(2,1)S(1)}, bf16[40,4096]{1,0:T(8,128)(2,1)S(1)}, u32[]{:S(2)}, u32[]{:S(2)}) collective-permute-start(bf16[40,4096]{1,0:T(8,128)(2,1)S(1)} %get-tuple-element.51), channel_id=1, source_target_pairs={{0,2},{2,4},{4,6},{6,0},{1,3},{3,5},{5,7},{7,1},{8,10},{10,12},{12... | collective-permute-start | bytes 983048 | tf_op jit(solution)/shard_map/ppermute | solution.py:331
  178.9 4.6 %collective-permute-start.18 = (bf16[40,4096]{1,0:T(8,128)(2,1)S(1)}, bf16[40,4096]{1,0:T(8,128)(2,1)S(1)}, u32[]{:S(2)}, u32[]{:S(2)}) collective-permute-start(bf16[40,4096]{1,0:T(8,128)(2,1)S(1)} %get-tuple-element.53), channel_id=1, source_target_pairs={{0,4},{2,6},{4,0},{6,2},{1,5},{3,7},{5,1},{7,3},{8,12},{10,14},{12... | collective-permute-start | bytes 983048 | tf_op jit(solution)/shard_map/ppermute | solution.py:331
  183.5 3.0 %collective-permute-start.19 = (bf16[40,4096]{1,0:T(8,128)(2,1)S(1)}, bf16[40,4096]{1,0:T(8,128)(2,1)S(1)}, u32[]{:S(2)}, u32[]{:S(2)}) collective-permute-start(bf16[40,4096]{1,0:T(8,128)(2,1)S(1)} %get-tuple-element.52), channel_id=1, source_target_pairs={{0,6},{2,0},{4,2},{6,4},{1,7},{3,1},{5,3},{7,5},{8,14},{10,8},{12,... | collective-permute-start | bytes 983048 | tf_op jit(solution)/shard_map/ppermute | solution.py:331
  186.5 2.3 %collective-permute-done.17 = bf16[40,4096]{1,0:T(8,128)(2,1)S(1)} collective-permute-done((bf16[40,4096]{1,0:T(8,128)(2,1)S(1)}, bf16[40,4096]{1,0:T(8,128)(2,1)S(1)}, u32[]{:S(2)}, u32[]{:S(2)}) %collective-permute-start.17) | collective-permute-done | bytes 327712 | tf_op jit(solution)/shard_map/ppermute | solution.py:331
  188.9 7.1 %collective-permute-done.18 = bf16[40,4096]{1,0:T(8,128)(2,1)S(1)} collective-permute-done((bf16[40,4096]{1,0:T(8,128)(2,1)S(1)}, bf16[40,4096]{1,0:T(8,128)(2,1)S(1)}, u32[]{:S(2)}, u32[]{:S(2)}) %collective-permute-start.18) | collective-permute-done | bytes 327712 | tf_op jit(solution)/shard_map/ppermute | solution.py:331
  196.0 2.2 %collective-permute-done.19 = bf16[40,4096]{1,0:T(8,128)(2,1)S(1)} collective-permute-done((bf16[40,4096]{1,0:T(8,128)(2,1)S(1)}, bf16[40,4096]{1,0:T(8,128)(2,1)S(1)}, u32[]{:S(2)}, u32[]{:S(2)}) %collective-permute-start.19) | collective-permute-done | bytes 327712 | tf_op jit(solution)/shard_map/ppermute | solution.py:331
  (100 shorter events, 12.4 us)
Async XLA Ops:
  3.6 61.7 %collective-permute-start = (bf16[320,256]{1,0:T(8,128)(2,1)}, bf16[320,256]{1,0:T(8,128)(2,1)S(1)}, u32[]{:S(2)}, u32[]{:S(2)}) collective-permute-start(bf16[320,256]{1,0:T(8,128)(2,1)} %shard_map.109.refs_4_), channel_id=1, source_target_pairs={{0,32},{32,64},{64,96},{96,128},{128,160},{160,192},{192,224},{224... | collective-permute-start | bytes 491528 | tf_op jit(solution)/shard_map/ppermute | solution.py:238
  16.7 48.7 %collective-permute-start.1 = (bf16[320,256]{1,0:T(8,128)(2,1)}, bf16[320,256]{1,0:T(8,128)(2,1)S(1)}, u32[]{:S(2)}, u32[]{:S(2)}) collective-permute-start(bf16[320,256]{1,0:T(8,128)(2,1)} %shard_map.109.refs_4_), channel_id=1, source_target_pairs={{32,0},{64,32},{96,64},{128,96},{160,128},{192,160},{224,192},{0,2... | collective-permute-start | bytes 491528 | tf_op jit(solution)/shard_map/ppermute | solution.py:239
  52.4 13.0 %copy-start = (bf16[320,128]{1,0:T(8,128)(2,1)S(1)}, bf16[320,128]{1,0:T(8,128)(2,1)}, u32[]{:S(2)}) copy-start(bf16[320,128]{1,0:T(8,128)(2,1)} %param.12) | copy-start | bytes 245764
  52.4 13.0 %copy-start.1 = (bf16[320,128]{1,0:T(8,128)(2,1)S(1)}, bf16[320,128]{1,0:T(8,128)(2,1)}, u32[]{:S(2)}) copy-start(bf16[320,128]{1,0:T(8,128)(2,1)} %param.13) | copy-start | bytes 245764
  52.4 17.0 %copy-start.5 = (bf16[320,256]{1,0:T(8,128)(2,1)S(1)}, bf16[320,256]{1,0:T(8,128)(2,1)}, u32[]{:S(2)}) copy-start(bf16[320,256]{1,0:T(8,128)(2,1)} %param.11) | copy-start | bytes 491524
  53.7 28.9 %copy-start.6 = (bf16[640,128]{1,0:T(8,128)(2,1)}, bf16[640,128]{1,0:T(8,128)(2,1)S(1)}, u32[]{:S(2)}) copy-start(bf16[640,128]{1,0:T(8,128)(2,1)S(1)} %pad_maximum_fusion.2.refs_0_) | copy-start | bytes 491524
  53.7 15.8 %collective-permute-start.2 = (bf16[640,128]{1,0:T(8,128)(2,1)S(1)}, bf16[640,128]{1,0:T(8,128)(2,1)S(1)}, u32[]{:S(2)}, u32[]{:S(2)}) collective-permute-start(bf16[640,128]{1,0:T(8,128)(2,1)S(1)} %pad_maximum_fusion.2.refs_0_), channel_id=1, source_target_pairs={{0,8},{8,16},{16,24},{24,0},{1,9},{9,17},{17,25},{25,1},{2,10},{10... | collective-permute-start | bytes 491528 | tf_op jit(solution)/shard_map/ppermute | solution.py:242
  57.2 17.2 %collective-permute-start.3 = (bf16[640,128]{1,0:T(8,128)(2,1)S(1)}, bf16[640,128]{1,0:T(8,128)(2,1)S(1)}, u32[]{:S(2)}, u32[]{:S(2)}) collective-permute-start(bf16[640,128]{1,0:T(8,128)(2,1)S(1)} %pad_maximum_fusion.2.refs_0_), channel_id=1, source_target_pairs={{0,16},{8,24},{16,0},{24,8},{1,17},{9,25},{17,1},{25,9},{2,18},{10... | collective-permute-start | bytes 491528 | tf_op jit(solution)/shard_map/ppermute | solution.py:242
  62.1 20.5 %collective-permute-start.4 = (bf16[640,128]{1,0:T(8,128)(2,1)S(1)}, bf16[640,128]{1,0:T(8,128)(2,1)S(1)}, u32[]{:S(2)}, u32[]{:S(2)}) collective-permute-start(bf16[640,128]{1,0:T(8,128)(2,1)S(1)} %pad_maximum_fusion.2.refs_0_), channel_id=1, source_target_pairs={{0,24},{8,0},{16,8},{24,16},{1,25},{9,1},{17,9},{25,17},{2,26},{10... | collective-permute-start | bytes 491528 | tf_op jit(solution)/shard_map/ppermute | solution.py:242
  65.4 17.2 %copy-start.13 = (bf16[320,256]{1,0:T(8,128)(2,1)}, bf16[320,256]{1,0:T(8,128)(2,1)S(1)}, u32[]{:S(2)}) copy-start(bf16[320,256]{1,0:T(8,128)(2,1)S(1)} %collective-permute-done.refs_5_) | copy-start | bytes 491524
  65.4 17.2 %copy-start.12 = (bf16[320,256]{1,0:T(8,128)(2,1)}, bf16[320,256]{1,0:T(8,128)(2,1)S(1)}, u32[]{:S(2)}) copy-start(bf16[320,256]{1,0:T(8,128)(2,1)S(1)} %collective-permute-done.1.refs_6_) | copy-start | bytes 491524
  65.5 24.1 %collective-permute-start.14 = (bf16[2,128,128]{2,1,0:T(8,128)(2,1)S(1)}, bf16[2,128,128]{2,1,0:T(8,128)(2,1)S(1)}, u32[]{:S(2)}, u32[]{:S(2)}) collective-permute-start(bf16[2,128,128]{2,1,0:T(8,128)(2,1)S(1)} %get-tuple-element.67), channel_id=1, source_target_pairs={{0,8},{8,16},{16,24},{24,32},{32,40},{40,48},{48,56},{56,64},{64,7... | collective-permute-start | bytes 196616 | tf_op jit(solution)/shard_map/ppermute | solution.py:272
  68.1 21.5 %collective-permute-start.15 = (bf16[2,128,128]{2,1,0:T(8,128)(2,1)S(1)}, bf16[2,128,128]{2,1,0:T(8,128)(2,1)S(1)}, u32[]{:S(2)}, u32[]{:S(2)}) collective-permute-start(bf16[2,128,128]{2,1,0:T(8,128)(2,1)S(1)} %get-tuple-element.66), channel_id=1, source_target_pairs={{8,0},{16,8},{24,16},{32,24},{40,32},{48,40},{56,48},{64,56},{72,6... | collective-permute-start | bytes 196616 | tf_op jit(solution)/shard_map/ppermute | solution.py:273
  69.5 13.1 %copy-start.16 = (bf16[640,128]{1,0:T(8,128)(2,1)}, bf16[640,128]{1,0:T(8,128)(2,1)S(1)}, u32[]{:S(2)}) copy-start(bf16[640,128]{1,0:T(8,128)(2,1)S(1)} %collective-permute-done.2.refs_1_) | copy-start | bytes 491524
  69.5 21.6 %collective-permute-start.5 = (bf16[320,256]{1,0:T(8,128)(2,1)S(1)}, bf16[320,256]{1,0:T(8,128)(2,1)S(1)}, u32[]{:S(2)}, u32[]{:S(2)}) collective-permute-start(bf16[320,256]{1,0:T(8,128)(2,1)S(1)} %collective-permute-done.refs_5_), channel_id=1, source_target_pairs={{0,32},{32,64},{64,96},{96,128},{128,160},{160,192},{192,224},{224... | collective-permute-start | bytes 491528 | tf_op jit(solution)/shard_map/ppermute | solution.py:252
  74.4 8.2 %copy-start.17 = (bf16[640,128]{1,0:T(8,128)(2,1)}, bf16[640,128]{1,0:T(8,128)(2,1)S(1)}, u32[]{:S(2)}) copy-start(bf16[640,128]{1,0:T(8,128)(2,1)S(1)} %collective-permute-done.3.refs_2_) | copy-start | bytes 491524
  74.4 18.7 %collective-permute-start.8 = (bf16[320,256]{1,0:T(8,128)(2,1)S(1)}, bf16[320,256]{1,0:T(8,128)(2,1)S(1)}, u32[]{:S(2)}, u32[]{:S(2)}) collective-permute-start(bf16[320,256]{1,0:T(8,128)(2,1)S(1)} %collective-permute-done.1.refs_6_), channel_id=1, source_target_pairs={{32,0},{64,32},{96,64},{128,96},{160,128},{192,160},{224,192},{0,2... | collective-permute-start | bytes 491528 | tf_op jit(solution)/shard_map/ppermute | solution.py:252
  91.1 9.7 %copy-start.14 = (bf16[320,256]{1,0:T(8,128)(2,1)}, bf16[320,256]{1,0:T(8,128)(2,1)S(1)}, u32[]{:S(2)}) copy-start(bf16[320,256]{1,0:T(8,128)(2,1)S(1)} %collective-permute-done.5.refs_1_) | copy-start | bytes 491524
  91.1 21.4 %collective-permute-start.6 = (bf16[320,256]{1,0:T(8,128)(2,1)S(1)}, bf16[320,256]{1,0:T(8,128)(2,1)S(1)}, u32[]{:S(2)}, u32[]{:S(2)}) collective-permute-start(bf16[320,256]{1,0:T(8,128)(2,1)S(1)} %collective-permute-done.5.refs_1_), channel_id=1, source_target_pairs={{0,32},{32,64},{64,96},{96,128},{128,160},{160,192},{192,224},{224... | collective-permute-start | bytes 491528 | tf_op jit(solution)/shard_map/ppermute | solution.py:252
  93.1 10.1 %collective-permute-start.9 = (bf16[320,256]{1,0:T(8,128)(2,1)S(1)}, bf16[320,256]{1,0:T(8,128)(2,1)S(1)}, u32[]{:S(2)}, u32[]{:S(2)}) collective-permute-start(bf16[320,256]{1,0:T(8,128)(2,1)S(1)} %collective-permute-done.8.refs_2_), channel_id=1, source_target_pairs={{32,0},{64,32},{96,64},{128,96},{160,128},{192,160},{224,192},{0,2... | collective-permute-start | bytes 491528 | tf_op jit(solution)/shard_map/ppermute | solution.py:252
  103.2 17.1 %copy-start.10 = (bf16[320,256]{1,0:T(8,128)(2,1)}, bf16[320,256]{1,0:T(8,128)(2,1)S(1)}, u32[]{:S(2)}) copy-start(bf16[320,256]{1,0:T(8,128)(2,1)S(1)} %collective-permute-done.9.refs_2_) | copy-start | bytes 491524
  103.2 22.7 %collective-permute-start.10 = (bf16[320,128]{1,0:T(8,128)(2,1)S(1)}, bf16[320,128]{1,0:T(8,128)(2,1)S(1)}, u32[]{:S(2)}, u32[]{:S(2)}) collective-permute-start(bf16[320,128]{1,0:T(8,128)(2,1)S(1)} %slice.143), channel_id=1, source_target_pairs={{32,0},{64,32},{96,64},{128,96},{160,128},{192,160},{224,192},{0,2... | collective-permute-start | bytes 245768 | tf_op jit(solution)/shard_map/ppermute | solution.py:252
  112.5 7.7 %copy-start.9 = (bf16[320,256]{1,0:T(8,128)(2,1)}, bf16[320,256]{1,0:T(8,128)(2,1)S(1)}, u32[]{:S(2)}) copy-start(bf16[320,256]{1,0:T(8,128)(2,1)S(1)} %collective-permute-done.6.refs_1_) | copy-start | bytes 491524
  112.6 13.3 %collective-permute-start.7 = (bf16[320,128]{1,0:T(8,128)(2,1)S(1)}, bf16[320,128]{1,0:T(8,128)(2,1)S(1)}, u32[]{:S(2)}, u32[]{:S(2)}) collective-permute-start(bf16[320,128]{1,0:T(8,128)(2,1)S(1)} %slice.142), channel_id=1, source_target_pairs={{0,32},{32,64},{64,96},{96,128},{128,160},{160,192},{192,224},{224... | collective-permute-start | bytes 245768 | tf_op jit(solution)/shard_map/ppermute | solution.py:252
  130.7 20.3 %collective-permute-start.11 = (bf16[144,640]{1,0:T(8,128)(2,1)}, bf16[144,640]{1,0:T(8,128)(2,1)S(1)}, u32[]{:S(2)}, u32[]{:S(2)}) collective-permute-start(bf16[144,640]{1,0:T(8,128)(2,1)} %get-tuple-element.43), channel_id=1, source_target_pairs={{0,24},{8,0},{16,8},{24,16},{1,25},{9,1},{17,9},{25,17},{2,26},{10... | collective-permute-start | bytes 552968 | tf_op jit(solution)/shard_map/ppermute | solution.py:261
  142.7 18.9 %collective-permute-start.12 = (bf16[144,640]{1,0:T(8,128)(2,1)}, bf16[144,640]{1,0:T(8,128)(2,1)S(1)}, u32[]{:S(2)}, u32[]{:S(2)}) collective-permute-start(bf16[144,640]{1,0:T(8,128)(2,1)} %get-tuple-element.44), channel_id=1, source_target_pairs={{0,16},{8,24},{16,0},{24,8},{1,17},{9,25},{17,1},{25,9},{2,18},{10... | collective-permute-start | bytes 552968 | tf_op jit(solution)/shard_map/ppermute | solution.py:261
  148.2 13.4 %collective-permute-start.13 = (bf16[144,640]{1,0:T(8,128)(2,1)}, bf16[144,640]{1,0:T(8,128)(2,1)S(1)}, u32[]{:S(2)}, u32[]{:S(2)}) collective-permute-start(bf16[144,640]{1,0:T(8,128)(2,1)} %get-tuple-element.45), channel_id=1, source_target_pairs={{0,8},{8,16},{16,24},{24,0},{1,9},{9,17},{17,25},{25,1},{2,10},{10... | collective-permute-start | bytes 552968 | tf_op jit(solution)/shard_map/ppermute | solution.py:261
  151.0 10.6 %copy-start.2 = (bf16[144,640]{1,0:T(8,128)(2,1)}, bf16[144,640]{1,0:T(8,128)(2,1)S(1)}, u32[]{:S(2)}) copy-start(bf16[144,640]{1,0:T(8,128)(2,1)S(1)} %collective-permute-done.11.refs_1_) | copy-start | bytes 552964
  168.0 7.1 %collective-permute-start.16 = (bf16[160,4096]{1,0:T(8,128)(2,1)}, bf16[160,4096]{1,0:T(8,128)(2,1)S(1)}, u32[]{:S(2)}, u32[]{:S(2)}) collective-permute-start(bf16[160,4096]{1,0:T(8,128)(2,1)} %get-tuple-element.50), channel_id=1, source_target_pairs={{0,1},{1,0},{2,3},{3,2},{4,5},{5,4},{6,7},{7,6},{8,9},{9,8},{10,11... | collective-permute-start | bytes 3932168 | tf_op jit(solution)/shard_map/ppermute | solution.py:326
  176.8 12.0 %collective-permute-start.17 = (bf16[40,4096]{1,0:T(8,128)(2,1)S(1)}, bf16[40,4096]{1,0:T(8,128)(2,1)S(1)}, u32[]{:S(2)}, u32[]{:S(2)}) collective-permute-start(bf16[40,4096]{1,0:T(8,128)(2,1)S(1)} %get-tuple-element.51), channel_id=1, source_target_pairs={{0,2},{2,4},{4,6},{6,0},{1,3},{3,5},{5,7},{7,1},{8,10},{10,12},{12... | collective-permute-start | bytes 983048 | tf_op jit(solution)/shard_map/ppermute | solution.py:331
  178.9 17.1 %collective-permute-start.18 = (bf16[40,4096]{1,0:T(8,128)(2,1)S(1)}, bf16[40,4096]{1,0:T(8,128)(2,1)S(1)}, u32[]{:S(2)}, u32[]{:S(2)}) collective-permute-start(bf16[40,4096]{1,0:T(8,128)(2,1)S(1)} %get-tuple-element.53), channel_id=1, source_target_pairs={{0,4},{2,6},{4,0},{6,2},{1,5},{3,7},{5,1},{7,3},{8,12},{10,14},{12... | collective-permute-start | bytes 983048 | tf_op jit(solution)/shard_map/ppermute | solution.py:331
  183.5 14.7 %collective-permute-start.19 = (bf16[40,4096]{1,0:T(8,128)(2,1)S(1)}, bf16[40,4096]{1,0:T(8,128)(2,1)S(1)}, u32[]{:S(2)}, u32[]{:S(2)}) collective-permute-start(bf16[40,4096]{1,0:T(8,128)(2,1)S(1)} %get-tuple-element.52), channel_id=1, source_target_pairs={{0,6},{2,0},{4,2},{6,4},{1,7},{3,1},{5,3},{7,5},{8,14},{10,8},{12,... | collective-permute-start | bytes 983048 | tf_op jit(solution)/shard_map/ppermute | solution.py:331
  (7 other events, 11.7 us)

commit v2 on v1

--- a/solution.py
+++ b/solution.py
@@ -19,6 +19,9 @@
 CORES = 2
 PLANES = 4
 TAIL = 16
+TURN_VMEM = 8 << 20
+ATTEND_VMEM = 24 << 20
+PROJECT_VMEM = 24 << 20
 
 
 def turn_tables(offset, local_rows):
@@ -59,6 +62,7 @@
     return pl.pallas_call(
         turn_kernel,
         out_shape=jax.ShapeDtypeStruct((rows, width), jnp.bfloat16),
+        compiler_params=pltpu.CompilerParams(vmem_limit_bytes=TURN_VMEM),
         cost_estimate=pl.CostEstimate(
             flops=rows * width * 16, bytes_accessed=rows * width * 8, transcendentals=rows
         ),
@@ -166,6 +170,7 @@
             attend_kernel, planes=len(queries), pieces=pieces, last=parts > 0, chunk=chunk
         ),
         out_shape=out_shape,
+        compiler_params=pltpu.CompilerParams(vmem_limit_bytes=ATTEND_VMEM),
         cost_estimate=pl.CostEstimate(
             flops=4 * rows * keys * HEAD,
             bytes_accessed=rows * HEAD * 10,
@@ -220,7 +225,9 @@
         out_specs=[pl.BlockSpec((rows // CORES, columns), lambda j: (0, j))] * CORES,
         out_shape=(half,) * CORES,
         scratch_shapes=[pltpu.VMEM((rows, grid_width), jnp.bfloat16)],
-        compiler_params=pltpu.CompilerParams(dimension_semantics=("arbitrary",)),
+        compiler_params=pltpu.CompilerParams(
+            dimension_semantics=("arbitrary",), vmem_limit_bytes=PROJECT_VMEM
+        ),
         cost_estimate=pl.CostEstimate(
             flops=2 * rows * (width + grid_width) * total,
             bytes_accessed=2 * total * (width + grid_width + rows),

time: 200 us -> 187 us (0.935)
  Pallas kernels: 31.4 us -> 14.8 us
  starting transfers between devices: 129 us -> 132 us
    pallas_call x4, Pallas kernels: 21.6 us -> 11.4 us  [attend(): pl.pallas_call(functools.partial(attend_kernel, planes=len(queries), piec...]
    ppermute x3, starting transfers between devices: 24.8 us -> 19.8 us  [grid_attend(): lax.ppermute(next_behind, 'hi', back)]
    ppermute x1, starting transfers between devices: 4.2 us -> 8.86 us  [sent_and_summed(): theirs = lax.ppermute(there, 'core', [(0, 1), (1, 0)])]
    ppermute x3, waiting for transfers between devices: 10.6 us -> 6.79 us  [grid_attend(): lax.ppermute(parts[d], 'lo', [(i, (i - d) % low) for i in range(low)])]
    pallas_call x2, Pallas kernels: 4.22 us -> 0.67 us  [turn(): pl.pallas_call(turn_kernel, out_shape=jax.ShapeDtypeStruct((rows, width),...]
    pallas_call x1, Pallas kernels: 5.65 us -> 2.75 us  [project(): pl.pallas_call(functools.partial(project_kernel, count=len(parts)), grid=...]
    ppermute x3, waiting for transfers between devices: 2.1 us -> 4.84 us  [grid_attend(): lax.ppermute(next_behind, 'hi', back)]
    ppermute x3, starting transfers between devices: 8.97 us -> 11.2 us  [grid_attend(): lax.ppermute(next_ahead, 'hi', ring)]
  transfers between devices with their start and end apart: 20 -> 20, of which waited for: 6 -> 8; matrix products, arithmetic and copies ran while one was open for 2% -> 3% of each run, Pallas kernels for 10% -> 5%
where the time goes in v2:
time: 187 us; the launch traced here: 186 us
  starting transfers between devices  132 us (71%)
  waiting for transfers between devices  25.5 us (14%)
  Pallas kernels  14.8 us (8%)
  other arithmetic  6.47 us (3%)
  local copies, waits for them, and re-layouts  4.68 us (3%)
    ppermute x1, starting transfers between devices, grid_attend(): behind = lax.ppermute(kv, 'hi', back)  33.5 us
    ppermute x3, starting transfers between devices, grid_attend(): lax.ppermute(parts[d], 'lo', [(i, (i - d) % low) for i in range(low)])  20.3 us
    ppermute x3, starting transfers between devices, grid_attend(): lax.ppermute(next_behind, 'hi', back)  19.8 us
    ppermute x1, starting transfers between devices, grid_attend(): ahead = lax.ppermute(kv, 'hi', ring)  13.1 us
    pallas_call x4, Pallas kernels, attend(): pl.pallas_call(functools.partial(attend_kernel, planes=len(queries), piec...  11.4 us
    ppermute x3, waiting for transfers between devices, sent_and_summed(): lax.ppermute(tiles[d], 'x', [(i, (i + d) % across) for i in range(across)])  11.2 us
    ppermute x3, starting transfers between devices, grid_attend(): lax.ppermute(next_ahead, 'hi', ring)  11.2 us
    ppermute x3, starting transfers between devices, grid_attend(): lax.ppermute(queries, 'lo', [(i, (i + d) % low) for i in range(low)])  11.1 us
  transfers between devices with their start and end apart: 20, of which 8 were waited for; matrix products, arithmetic and copies ran while one was open for 3% of the time, Pallas kernels for 5%

profile of v2, /device:TPU:33, one launch (start us, length us, event | category | flops | bytes accessed | tf_op | source)
XLA Modules:
  0.0 185.5 jit_solution(14457707880079130470)
XLA Ops:
  3.6 13.1 %collective-permute-start = (bf16[320,256]{1,0:T(8,128)(2,1)S(1)}, bf16[320,256]{1,0:T(8,128)(2,1)S(1)}, u32[]{:S(2)}, u32[]{:S(2)}) collective-permute-start(bf16[320,256]{1,0:T(8,128)(2,1)S(1)} %shard_map.109.refs_4_), channel_id=1, source_target_pairs={{0,32},{32,64},{64,96},{96,128},{128,160},{160,192},{192,224},{224... | collective-permute-start | bytes 491528 | tf_op jit(solution)/shard_map/ppermute | solution.py:245
  16.7 33.5 %collective-permute-start.1 = (bf16[320,256]{1,0:T(8,128)(2,1)S(1)}, bf16[320,256]{1,0:T(8,128)(2,1)S(1)}, u32[]{:S(2)}, u32[]{:S(2)}) collective-permute-start(bf16[320,256]{1,0:T(8,128)(2,1)S(1)} %shard_map.109.refs_4_), channel_id=1, source_target_pairs={{32,0},{64,32},{96,64},{128,96},{160,128},{192,160},{224,192},{0,2... | collective-permute-start | bytes 491528 | tf_op jit(solution)/shard_map/ppermute | solution.py:246
  50.9 3.5 %collective-permute-start.2 = (bf16[640,128]{1,0:T(8,128)(2,1)S(1)}, bf16[640,128]{1,0:T(8,128)(2,1)S(1)}, u32[]{:S(2)}, u32[]{:S(2)}) collective-permute-start(bf16[640,128]{1,0:T(8,128)(2,1)S(1)} %pad_maximum_fusion.2.refs_0_), channel_id=1, source_target_pairs={{0,8},{8,16},{16,24},{24,0},{1,9},{9,17},{17,25},{25,1},{2,10},{10... | collective-permute-start | bytes 491528 | tf_op jit(solution)/shard_map/ppermute | solution.py:249
  54.4 4.8 %collective-permute-start.3 = (bf16[640,128]{1,0:T(8,128)(2,1)S(1)}, bf16[640,128]{1,0:T(8,128)(2,1)S(1)}, u32[]{:S(2)}, u32[]{:S(2)}) collective-permute-start(bf16[640,128]{1,0:T(8,128)(2,1)S(1)} %pad_maximum_fusion.2.refs_0_), channel_id=1, source_target_pairs={{0,16},{8,24},{16,0},{24,8},{1,17},{9,25},{17,1},{25,9},{2,18},{10... | collective-permute-start | bytes 491528 | tf_op jit(solution)/shard_map/ppermute | solution.py:249
  59.3 2.7 %collective-permute-start.4 = (bf16[640,128]{1,0:T(8,128)(2,1)S(1)}, bf16[640,128]{1,0:T(8,128)(2,1)S(1)}, u32[]{:S(2)}, u32[]{:S(2)}) collective-permute-start(bf16[640,128]{1,0:T(8,128)(2,1)S(1)} %pad_maximum_fusion.2.refs_0_), channel_id=1, source_target_pairs={{0,24},{8,0},{16,8},{24,16},{1,25},{9,1},{17,9},{25,17},{2,26},{10... | collective-permute-start | bytes 491528 | tf_op jit(solution)/shard_map/ppermute | solution.py:249
  64.7 3.2 %collective-permute-start.14 = (bf16[2,128,128]{2,1,0:T(8,128)(2,1)}, bf16[2,128,128]{2,1,0:T(8,128)(2,1)}, u32[]{:S(2)}, u32[]{:S(2)}) collective-permute-start(bf16[2,128,128]{2,1,0:T(8,128)(2,1)} %get-tuple-element.67), channel_id=1, source_target_pairs={{0,8},{8,16},{16,24},{24,32},{32,40},{40,48},{48,56},{56,64},{64,7... | collective-permute-start | bytes 196616 | tf_op jit(solution)/shard_map/ppermute | solution.py:279
  69.9 5.6 %collective-permute-start.5 = (bf16[320,256]{1,0:T(8,128)(2,1)S(1)}, bf16[320,256]{1,0:T(8,128)(2,1)S(1)}, u32[]{:S(2)}, u32[]{:S(2)}) collective-permute-start(bf16[320,256]{1,0:T(8,128)(2,1)S(1)} %collective-permute-done.refs_5_), channel_id=1, source_target_pairs={{0,32},{32,64},{64,96},{96,128},{128,160},{160,192},{192,224},{224... | collective-permute-start | bytes 491528 | tf_op jit(solution)/shard_map/ppermute | solution.py:259
  75.6 6.7 %collective-permute-start.8 = (bf16[320,256]{1,0:T(8,128)(2,1)S(1)}, bf16[320,256]{1,0:T(8,128)(2,1)S(1)}, u32[]{:S(2)}, u32[]{:S(2)}) collective-permute-start(bf16[320,256]{1,0:T(8,128)(2,1)S(1)} %collective-permute-done.1.refs_6_), channel_id=1, source_target_pairs={{32,0},{64,32},{96,64},{128,96},{160,128},{192,160},{224,192},{0,2... | collective-permute-start | bytes 491528 | tf_op jit(solution)/shard_map/ppermute | solution.py:259
  82.3 4.1 %shard_map.111 = (f32[1,2560]{1,0:T(1,128)S(1)}, f32[1,2560]{1,0:T(1,128)S(1)}, f32[128,2560]{1,0:T(8,128)S(1)}, bf16[2560,128]{1,0:T(8,128)(2,1)S(1)}) custom-call(bf16[640,128]{1,0:T(8,128)(2,1)S(1)} %pad_maximum_fusion.2.refs_0_, bf16[640,128]{1,0:T(8,128)(2,1)S(1)} %collective-permute-done.2.refs_1_, ...), custom_call_target="tpu_custom_call" | custom-call | flops 1258291200 | bytes 3276800 | tf_op jit(solution)/shard_map/pallas_call | solution.py:168
  89.6 2.5 %collective-permute-start.6 = (bf16[320,256]{1,0:T(8,128)(2,1)S(1)}, bf16[320,256]{1,0:T(8,128)(2,1)S(1)}, u32[]{:S(2)}, u32[]{:S(2)}) collective-permute-start(bf16[320,256]{1,0:T(8,128)(2,1)S(1)} %collective-permute-done.5.refs_1_), channel_id=1, source_target_pairs={{0,32},{32,64},{64,96},{96,128},{128,160},{160,192},{192,224},{224... | collective-permute-start | bytes 491528 | tf_op jit(solution)/shard_map/ppermute | solution.py:259
  92.1 6.7 %collective-permute-start.9 = (bf16[320,256]{1,0:T(8,128)(2,1)S(1)}, bf16[320,256]{1,0:T(8,128)(2,1)S(1)}, u32[]{:S(2)}, u32[]{:S(2)}) collective-permute-start(bf16[320,256]{1,0:T(8,128)(2,1)S(1)} %collective-permute-done.8.refs_2_), channel_id=1, source_target_pairs={{32,0},{64,32},{96,64},{128,96},{160,128},{192,160},{224,192},{0,2... | collective-permute-start | bytes 491528 | tf_op jit(solution)/shard_map/ppermute | solution.py:259
  99.5 2.9 %collective-permute-done.9.refs_2_ = bf16[320,256]{1,0:T(8,128)(2,1)S(1)} collective-permute-done((bf16[320,256]{1,0:T(8,128)(2,1)S(1)}, bf16[320,256]{1,0:T(8,128)(2,1)S(1)}, u32[]{:S(2)}, u32[]{:S(2)}) %collective-permute-start.9) | collective-permute-done | bytes 163872 | tf_op jit(solution)/shard_map/ppermute | solution.py:259
  102.4 6.4 %collective-permute-start.10 = (bf16[320,128]{1,0:T(8,128)(2,1)S(1)}, bf16[320,128]{1,0:T(8,128)(2,1)S(1)}, u32[]{:S(2)}, u32[]{:S(2)}) collective-permute-start(bf16[320,128]{1,0:T(8,128)(2,1)S(1)} %slice.143), channel_id=1, source_target_pairs={{32,0},{64,32},{96,64},{128,96},{160,128},{192,160},{224,192},{0,2... | collective-permute-start | bytes 245768 | tf_op jit(solution)/shard_map/ppermute | solution.py:259
  108.9 3.0 %collective-permute-start.7 = (bf16[320,128]{1,0:T(8,128)(2,1)S(1)}, bf16[320,128]{1,0:T(8,128)(2,1)S(1)}, u32[]{:S(2)}, u32[]{:S(2)}) collective-permute-start(bf16[320,128]{1,0:T(8,128)(2,1)S(1)} %slice.142), channel_id=1, source_target_pairs={{0,32},{32,64},{64,96},{96,128},{128,160},{160,192},{192,224},{224... | collective-permute-start | bytes 245768 | tf_op jit(solution)/shard_map/ppermute | solution.py:259
  111.9 2.8 %shard_map.112 = (f32[1,2560]{1,0:T(1,128)S(1)}, f32[1,2560]{1,0:T(1,128)S(1)}, f32[128,2560]{1,0:T(8,128)S(1)}) custom-call(bf16[2560,128]{1,0:T(8,128)(2,1)S(1)} %get-tuple-element.32.refs_0_, bf16[320,256]{1,0:T(8,128)(2,1)S(1)} %collective-permute-done.5.refs_1_, bf16[320,256]{1,0:T(8,128)(2,1)S(1)} %collective-permute-done.8.refs_2_, ...), custom_call_target="tpu_custom_call" | custom-call | flops 838860800 | bytes 3276800 | tf_op jit(solution)/shard_map/pallas_call | solution.py:168
  114.7 2.8 %shard_map.113 = (f32[1,2560]{1,0:T(1,128)S(1)}, f32[1,2560]{1,0:T(1,128)S(1)}, f32[128,2560]{1,0:T(8,128)S(1)}) custom-call(bf16[2560,128]{1,0:T(8,128)(2,1)S(1)} %get-tuple-element.32.refs_0_, bf16[320,256]{1,0:T(8,128)(2,1)S(1)} %collective-permute-done.6.refs_1_, bf16[320,256]{1,0:T(8,128)(2,1)S(1)} %collective-permute-done.9.refs_2_, ...), custom_call_target="tpu_custom_call" | custom-call | flops 838860800 | bytes 3276800 | tf_op jit(solution)/shard_map/pallas_call | solution.py:168
  117.5 2.0 %collective-permute-done.10.refs_2_ = bf16[320,128]{1,0:T(8,128)(2,1)S(1)} collective-permute-done((bf16[320,128]{1,0:T(8,128)(2,1)S(1)}, bf16[320,128]{1,0:T(8,128)(2,1)S(1)}, u32[]{:S(2)}, u32[]{:S(2)}) %collective-permute-start.10) | collective-permute-done | bytes 81952 | tf_op jit(solution)/shard_map/ppermute | solution.py:259
  119.5 1.7 shard_map.114
  121.2 14.5 %collective-permute-start.11 = (bf16[144,640]{1,0:T(8,128)(2,1)S(1)}, bf16[144,640]{1,0:T(8,128)(2,1)S(1)}, u32[]{:S(2)}, u32[]{:S(2)}) collective-permute-start(bf16[144,640]{1,0:T(8,128)(2,1)S(1)} %get-tuple-element.43), channel_id=1, source_target_pairs={{0,24},{8,0},{16,8},{24,16},{1,25},{9,1},{17,9},{25,17},{2,26},{10... | collective-permute-start | bytes 552968 | tf_op jit(solution)/shard_map/ppermute | solution.py:268
  135.7 3.9 %collective-permute-start.12 = (bf16[144,640]{1,0:T(8,128)(2,1)S(1)}, bf16[144,640]{1,0:T(8,128)(2,1)S(1)}, u32[]{:S(2)}, u32[]{:S(2)}) collective-permute-start(bf16[144,640]{1,0:T(8,128)(2,1)S(1)} %get-tuple-element.44), channel_id=1, source_target_pairs={{0,16},{8,24},{16,0},{24,8},{1,17},{9,25},{17,1},{25,9},{2,18},{10... | collective-permute-start | bytes 552968 | tf_op jit(solution)/shard_map/ppermute | solution.py:268
  139.6 2.0 %collective-permute-start.13 = (bf16[144,640]{1,0:T(8,128)(2,1)S(1)}, bf16[144,640]{1,0:T(8,128)(2,1)S(1)}, u32[]{:S(2)}, u32[]{:S(2)}) collective-permute-start(bf16[144,640]{1,0:T(8,128)(2,1)S(1)} %get-tuple-element.45), channel_id=1, source_target_pairs={{0,8},{8,16},{16,24},{24,0},{1,9},{9,17},{17,25},{25,1},{2,10},{10... | collective-permute-start | bytes 552968 | tf_op jit(solution)/shard_map/ppermute | solution.py:268
  141.7 3.6 %collective-permute-done.12.refs_2_ = bf16[144,640]{1,0:T(8,128)(2,1)S(1)} collective-permute-done((bf16[144,640]{1,0:T(8,128)(2,1)S(1)}, bf16[144,640]{1,0:T(8,128)(2,1)S(1)}, u32[]{:S(2)}, u32[]{:S(2)}) %collective-permute-start.12) | collective-permute-done | bytes 184352 | tf_op jit(solution)/shard_map/ppermute | solution.py:268
  145.4 3.2 %collective-permute-done.13.refs_3_ = bf16[144,640]{1,0:T(8,128)(2,1)S(1)} collective-permute-done((bf16[144,640]{1,0:T(8,128)(2,1)S(1)}, bf16[144,640]{1,0:T(8,128)(2,1)S(1)}, u32[]{:S(2)}, u32[]{:S(2)}) %collective-permute-start.13) | collective-permute-done | bytes 184352 | tf_op jit(solution)/shard_map/ppermute | solution.py:268
  148.5 2.8 %shard_map.115 = (bf16[160,4096]{1,0:T(8,128)(2,1)S(1)}, bf16[160,4096]{1,0:T(8,128)(2,1)S(1)}) custom-call(bf16[144,640]{1,0:T(8,128)(2,1)S(1)} %get-tuple-element.42.refs_0_, bf16[144,640]{1,0:T(8,128)(2,1)S(1)} %collective-permute-done.11.refs_1_, bf16[144,640]{1,0:T(8,128)(2,1)S(1)} %collective-permute-done.12.refs_2_, ...), custom_call_target="tpu_custom_call" | custom-call | flops 1342177280 | bytes 6815744 | tf_op jit(solution)/shard_map/pallas_call | solution.py:216
  151.3 8.9 %collective-permute-start.16 = (bf16[160,4096]{1,0:T(8,128)(2,1)S(1)}, bf16[160,4096]{1,0:T(8,128)(2,1)S(1)}, u32[]{:S(2)}, u32[]{:S(2)}) collective-permute-start(bf16[160,4096]{1,0:T(8,128)(2,1)S(1)} %get-tuple-element.50), channel_id=1, source_target_pairs={{0,1},{1,0},{2,3},{3,2},{4,5},{5,4},{6,7},{7,6},{8,9},{9,8},{10,11... | collective-permute-start | bytes 3932168 | tf_op jit(solution)/shard_map/ppermute | solution.py:333
  160.2 2.6 %collective-permute-done.16 = bf16[160,4096]{1,0:T(8,128)(2,1)S(1)} collective-permute-done((bf16[160,4096]{1,0:T(8,128)(2,1)S(1)}, bf16[160,4096]{1,0:T(8,128)(2,1)S(1)}, u32[]{:S(2)}, u32[]{:S(2)}) %collective-permute-start.16) | collective-permute-done | bytes 1310752 | tf_op jit(solution)/shard_map/ppermute | solution.py:333
  163.3 2.4 %collective-permute-start.17 = (bf16[40,4096]{1,0:T(8,128)(2,1)S(1)}, bf16[40,4096]{1,0:T(8,128)(2,1)S(1)}, u32[]{:S(2)}, u32[]{:S(2)}) collective-permute-start(bf16[40,4096]{1,0:T(8,128)(2,1)S(1)} %get-tuple-element.51), channel_id=1, source_target_pairs={{0,2},{2,4},{4,6},{6,0},{1,3},{3,5},{5,7},{7,1},{8,10},{10,12},{12... | collective-permute-start | bytes 983048 | tf_op jit(solution)/shard_map/ppermute | solution.py:338
  165.7 4.7 %collective-permute-start.18 = (bf16[40,4096]{1,0:T(8,128)(2,1)S(1)}, bf16[40,4096]{1,0:T(8,128)(2,1)S(1)}, u32[]{:S(2)}, u32[]{:S(2)}) collective-permute-start(bf16[40,4096]{1,0:T(8,128)(2,1)S(1)} %get-tuple-element.53), channel_id=1, source_target_pairs={{0,4},{2,6},{4,0},{6,2},{1,5},{3,7},{5,1},{7,3},{8,12},{10,14},{12... | collective-permute-start | bytes 983048 | tf_op jit(solution)/shard_map/ppermute | solution.py:338
  170.4 3.0 %collective-permute-start.19 = (bf16[40,4096]{1,0:T(8,128)(2,1)S(1)}, bf16[40,4096]{1,0:T(8,128)(2,1)S(1)}, u32[]{:S(2)}, u32[]{:S(2)}) collective-permute-start(bf16[40,4096]{1,0:T(8,128)(2,1)S(1)} %get-tuple-element.52), channel_id=1, source_target_pairs={{0,6},{2,0},{4,2},{6,4},{1,7},{3,1},{5,3},{7,5},{8,14},{10,8},{12,... | collective-permute-start | bytes 983048 | tf_op jit(solution)/shard_map/ppermute | solution.py:338
  173.4 1.9 %collective-permute-done.17 = bf16[40,4096]{1,0:T(8,128)(2,1)S(1)} collective-permute-done((bf16[40,4096]{1,0:T(8,128)(2,1)S(1)}, bf16[40,4096]{1,0:T(8,128)(2,1)S(1)}, u32[]{:S(2)}, u32[]{:S(2)}) %collective-permute-start.17) | collective-permute-done | bytes 327712 | tf_op jit(solution)/shard_map/ppermute | solution.py:338
  175.3 7.6 %collective-permute-done.18 = bf16[40,4096]{1,0:T(8,128)(2,1)S(1)} collective-permute-done((bf16[40,4096]{1,0:T(8,128)(2,1)S(1)}, bf16[40,4096]{1,0:T(8,128)(2,1)S(1)}, u32[]{:S(2)}, u32[]{:S(2)}) %collective-permute-start.18) | collective-permute-done | bytes 327712 | tf_op jit(solution)/shard_map/ppermute | solution.py:338
  182.9 1.7 collective-permute-done.19
  (92 shorter events, 14.0 us)
Async XLA Ops:
  0.0 50.2 %copy-start.2 = (bf16[320,256]{1,0:T(8,128)(2,1)S(1)}, bf16[320,256]{1,0:T(8,128)(2,1)}, u32[]{:S(2)}) copy-start(bf16[320,256]{1,0:T(8,128)(2,1)} %x_ref.2) | copy-start | bytes 491524
  0.0 50.2 %copy-start.6 = (f32[128]{0:T(128)S(1)}, f32[128]{0:T(128)}, u32[]{:S(2)}) copy-start(f32[128]{0:T(128)} %param.18) | copy-start | bytes 1540
  3.6 60.4 %collective-permute-start = (bf16[320,256]{1,0:T(8,128)(2,1)S(1)}, bf16[320,256]{1,0:T(8,128)(2,1)S(1)}, u32[]{:S(2)}, u32[]{:S(2)}) collective-permute-start(bf16[320,256]{1,0:T(8,128)(2,1)S(1)} %shard_map.109.refs_4_), channel_id=1, source_target_pairs={{0,32},{32,64},{64,96},{96,128},{128,160},{160,192},{192,224},{224... | collective-permute-start | bytes 491528 | tf_op jit(solution)/shard_map/ppermute | solution.py:245
  16.7 47.3 %collective-permute-start.1 = (bf16[320,256]{1,0:T(8,128)(2,1)S(1)}, bf16[320,256]{1,0:T(8,128)(2,1)S(1)}, u32[]{:S(2)}, u32[]{:S(2)}) collective-permute-start(bf16[320,256]{1,0:T(8,128)(2,1)S(1)} %shard_map.109.refs_4_), channel_id=1, source_target_pairs={{32,0},{64,32},{96,64},{128,96},{160,128},{192,160},{224,192},{0,2... | collective-permute-start | bytes 491528 | tf_op jit(solution)/shard_map/ppermute | solution.py:246
  50.6 13.3 %copy-start.8 = (bf16[320,128]{1,0:T(8,128)(2,1)S(1)}, bf16[320,128]{1,0:T(8,128)(2,1)}, u32[]{:S(2)}) copy-start(bf16[320,128]{1,0:T(8,128)(2,1)} %param.12) | copy-start | bytes 245764
  50.7 13.3 %copy-start.9 = (bf16[320,128]{1,0:T(8,128)(2,1)S(1)}, bf16[320,128]{1,0:T(8,128)(2,1)}, u32[]{:S(2)}) copy-start(bf16[320,128]{1,0:T(8,128)(2,1)} %param.13) | copy-start | bytes 245764
  50.7 18.5 %copy-start.13 = (bf16[320,256]{1,0:T(8,128)(2,1)S(1)}, bf16[320,256]{1,0:T(8,128)(2,1)}, u32[]{:S(2)}) copy-start(bf16[320,256]{1,0:T(8,128)(2,1)} %param.11) | copy-start | bytes 491524
  50.9 19.1 %collective-permute-start.2 = (bf16[640,128]{1,0:T(8,128)(2,1)S(1)}, bf16[640,128]{1,0:T(8,128)(2,1)S(1)}, u32[]{:S(2)}, u32[]{:S(2)}) collective-permute-start(bf16[640,128]{1,0:T(8,128)(2,1)S(1)} %pad_maximum_fusion.2.refs_0_), channel_id=1, source_target_pairs={{0,8},{8,16},{16,24},{24,0},{1,9},{9,17},{17,25},{25,1},{2,10},{10... | collective-permute-start | bytes 491528 | tf_op jit(solution)/shard_map/ppermute | solution.py:249
  54.4 21.2 %collective-permute-start.3 = (bf16[640,128]{1,0:T(8,128)(2,1)S(1)}, bf16[640,128]{1,0:T(8,128)(2,1)S(1)}, u32[]{:S(2)}, u32[]{:S(2)}) collective-permute-start(bf16[640,128]{1,0:T(8,128)(2,1)S(1)} %pad_maximum_fusion.2.refs_0_), channel_id=1, source_target_pairs={{0,16},{8,24},{16,0},{24,8},{1,17},{9,25},{17,1},{25,9},{2,18},{10... | collective-permute-start | bytes 491528 | tf_op jit(solution)/shard_map/ppermute | solution.py:249
  59.3 23.0 %collective-permute-start.4 = (bf16[640,128]{1,0:T(8,128)(2,1)S(1)}, bf16[640,128]{1,0:T(8,128)(2,1)S(1)}, u32[]{:S(2)}, u32[]{:S(2)}) collective-permute-start(bf16[640,128]{1,0:T(8,128)(2,1)S(1)} %pad_maximum_fusion.2.refs_0_), channel_id=1, source_target_pairs={{0,24},{8,0},{16,8},{24,16},{1,25},{9,1},{17,9},{25,17},{2,26},{10... | collective-permute-start | bytes 491528 | tf_op jit(solution)/shard_map/ppermute | solution.py:249
  64.7 21.7 %collective-permute-start.14 = (bf16[2,128,128]{2,1,0:T(8,128)(2,1)}, bf16[2,128,128]{2,1,0:T(8,128)(2,1)}, u32[]{:S(2)}, u32[]{:S(2)}) collective-permute-start(bf16[2,128,128]{2,1,0:T(8,128)(2,1)} %get-tuple-element.67), channel_id=1, source_target_pairs={{0,8},{8,16},{16,24},{24,32},{32,40},{40,48},{48,56},{56,64},{64,7... | collective-permute-start | bytes 196616 | tf_op jit(solution)/shard_map/ppermute | solution.py:279
  67.9 18.5 %collective-permute-start.15 = (bf16[2,128,128]{2,1,0:T(8,128)(2,1)}, bf16[2,128,128]{2,1,0:T(8,128)(2,1)}, u32[]{:S(2)}, u32[]{:S(2)}) collective-permute-start(bf16[2,128,128]{2,1,0:T(8,128)(2,1)} %get-tuple-element.66), channel_id=1, source_target_pairs={{8,0},{16,8},{24,16},{32,24},{40,32},{48,40},{56,48},{64,56},{72,6... | collective-permute-start | bytes 196616 | tf_op jit(solution)/shard_map/ppermute | solution.py:280
  69.9 16.5 %copy-start.10 = (bf16[320,128]{1,0:T(8,128)(2,1)S(1)}, bf16[320,128]{1,0:T(8,128)(2,1)}, u32[]{:S(2)}) copy-start(bf16[320,128]{1,0:T(8,128)(2,1)} %param.13) | copy-start | bytes 245764
  69.9 19.6 %collective-permute-start.5 = (bf16[320,256]{1,0:T(8,128)(2,1)S(1)}, bf16[320,256]{1,0:T(8,128)(2,1)S(1)}, u32[]{:S(2)}, u32[]{:S(2)}) collective-permute-start(bf16[320,256]{1,0:T(8,128)(2,1)S(1)} %collective-permute-done.refs_5_), channel_id=1, source_target_pairs={{0,32},{32,64},{64,96},{96,128},{128,160},{160,192},{192,224},{224... | collective-permute-start | bytes 491528 | tf_op jit(solution)/shard_map/ppermute | solution.py:259
  75.6 16.5 %collective-permute-start.8 = (bf16[320,256]{1,0:T(8,128)(2,1)S(1)}, bf16[320,256]{1,0:T(8,128)(2,1)S(1)}, u32[]{:S(2)}, u32[]{:S(2)}) collective-permute-start(bf16[320,256]{1,0:T(8,128)(2,1)S(1)} %collective-permute-done.1.refs_6_), channel_id=1, source_target_pairs={{32,0},{64,32},{96,64},{128,96},{160,128},{192,160},{224,192},{0,2... | collective-permute-start | bytes 491528 | tf_op jit(solution)/shard_map/ppermute | solution.py:259
  87.3 1.0 copy-start.7
  87.3 1.1 copy-start.11
  87.4 1.1 copy-start.12
  87.5 1.4 copy-start.14
  89.6 19.3 %collective-permute-start.6 = (bf16[320,256]{1,0:T(8,128)(2,1)S(1)}, bf16[320,256]{1,0:T(8,128)(2,1)S(1)}, u32[]{:S(2)}, u32[]{:S(2)}) collective-permute-start(bf16[320,256]{1,0:T(8,128)(2,1)S(1)} %collective-permute-done.5.refs_1_), channel_id=1, source_target_pairs={{0,32},{32,64},{64,96},{96,128},{128,160},{160,192},{192,224},{224... | collective-permute-start | bytes 491528 | tf_op jit(solution)/shard_map/ppermute | solution.py:259
  92.1 10.3 %collective-permute-start.9 = (bf16[320,256]{1,0:T(8,128)(2,1)S(1)}, bf16[320,256]{1,0:T(8,128)(2,1)S(1)}, u32[]{:S(2)}, u32[]{:S(2)}) collective-permute-start(bf16[320,256]{1,0:T(8,128)(2,1)S(1)} %collective-permute-done.8.refs_2_), channel_id=1, source_target_pairs={{32,0},{64,32},{96,64},{128,96},{160,128},{192,160},{224,192},{0,2... | collective-permute-start | bytes 491528 | tf_op jit(solution)/shard_map/ppermute | solution.py:259
  102.4 17.1 %collective-permute-start.10 = (bf16[320,128]{1,0:T(8,128)(2,1)S(1)}, bf16[320,128]{1,0:T(8,128)(2,1)S(1)}, u32[]{:S(2)}, u32[]{:S(2)}) collective-permute-start(bf16[320,128]{1,0:T(8,128)(2,1)S(1)} %slice.143), channel_id=1, source_target_pairs={{32,0},{64,32},{96,64},{128,96},{160,128},{192,160},{224,192},{0,2... | collective-permute-start | bytes 245768 | tf_op jit(solution)/shard_map/ppermute | solution.py:259
  108.9 10.6 %collective-permute-start.7 = (bf16[320,128]{1,0:T(8,128)(2,1)S(1)}, bf16[320,128]{1,0:T(8,128)(2,1)S(1)}, u32[]{:S(2)}, u32[]{:S(2)}) collective-permute-start(bf16[320,128]{1,0:T(8,128)(2,1)S(1)} %slice.142), channel_id=1, source_target_pairs={{0,32},{32,64},{64,96},{96,128},{128,160},{160,192},{192,224},{224... | collective-permute-start | bytes 245768 | tf_op jit(solution)/shard_map/ppermute | solution.py:259
  114.7 33.8 %copy-start.1 = (bf16[256,4096]{1,0:T(8,128)(2,1)S(1)}, bf16[256,4096]{1,0:T(8,128)(2,1)}, u32[]{:S(2)}) copy-start(bf16[256,4096]{1,0:T(8,128)(2,1)} %refs_6_.1) | copy-start | bytes 6291460
  119.5 29.1 %copy-start = (bf16[256,4096]{1,0:T(8,128)(2,1)S(1)}, bf16[256,4096]{1,0:T(8,128)(2,1)}, u32[]{:S(2)}) copy-start(bf16[256,4096]{1,0:T(8,128)(2,1)} %refs_5_.1) | copy-start | bytes 6291460
  121.2 20.5 %collective-permute-start.11 = (bf16[144,640]{1,0:T(8,128)(2,1)S(1)}, bf16[144,640]{1,0:T(8,128)(2,1)S(1)}, u32[]{:S(2)}, u32[]{:S(2)}) collective-permute-start(bf16[144,640]{1,0:T(8,128)(2,1)S(1)} %get-tuple-element.43), channel_id=1, source_target_pairs={{0,24},{8,0},{16,8},{24,16},{1,25},{9,1},{17,9},{25,17},{2,26},{10... | collective-permute-start | bytes 552968 | tf_op jit(solution)/shard_map/ppermute | solution.py:268
  135.7 9.7 %collective-permute-start.12 = (bf16[144,640]{1,0:T(8,128)(2,1)S(1)}, bf16[144,640]{1,0:T(8,128)(2,1)S(1)}, u32[]{:S(2)}, u32[]{:S(2)}) collective-permute-start(bf16[144,640]{1,0:T(8,128)(2,1)S(1)} %get-tuple-element.44), channel_id=1, source_target_pairs={{0,16},{8,24},{16,0},{24,8},{1,17},{9,25},{17,1},{25,9},{2,18},{10... | collective-permute-start | bytes 552968 | tf_op jit(solution)/shard_map/ppermute | solution.py:268
  139.6 8.9 %collective-permute-start.13 = (bf16[144,640]{1,0:T(8,128)(2,1)S(1)}, bf16[144,640]{1,0:T(8,128)(2,1)S(1)}, u32[]{:S(2)}, u32[]{:S(2)}) collective-permute-start(bf16[144,640]{1,0:T(8,128)(2,1)S(1)} %get-tuple-element.45), channel_id=1, source_target_pairs={{0,8},{8,16},{16,24},{24,0},{1,9},{9,17},{17,25},{25,1},{2,10},{10... | collective-permute-start | bytes 552968 | tf_op jit(solution)/shard_map/ppermute | solution.py:268
  151.3 11.5 %collective-permute-start.16 = (bf16[160,4096]{1,0:T(8,128)(2,1)S(1)}, bf16[160,4096]{1,0:T(8,128)(2,1)S(1)}, u32[]{:S(2)}, u32[]{:S(2)}) collective-permute-start(bf16[160,4096]{1,0:T(8,128)(2,1)S(1)} %get-tuple-element.50), channel_id=1, source_target_pairs={{0,1},{1,0},{2,3},{3,2},{4,5},{5,4},{6,7},{7,6},{8,9},{9,8},{10,11... | collective-permute-start | bytes 3932168 | tf_op jit(solution)/shard_map/ppermute | solution.py:333
  163.3 12.0 %collective-permute-start.17 = (bf16[40,4096]{1,0:T(8,128)(2,1)S(1)}, bf16[40,4096]{1,0:T(8,128)(2,1)S(1)}, u32[]{:S(2)}, u32[]{:S(2)}) collective-permute-start(bf16[40,4096]{1,0:T(8,128)(2,1)S(1)} %get-tuple-element.51), channel_id=1, source_target_pairs={{0,2},{2,4},{4,6},{6,0},{1,3},{3,5},{5,7},{7,1},{8,10},{10,12},{12... | collective-permute-start | bytes 983048 | tf_op jit(solution)/shard_map/ppermute | solution.py:338
  165.7 17.2 %collective-permute-start.18 = (bf16[40,4096]{1,0:T(8,128)(2,1)S(1)}, bf16[40,4096]{1,0:T(8,128)(2,1)S(1)}, u32[]{:S(2)}, u32[]{:S(2)}) collective-permute-start(bf16[40,4096]{1,0:T(8,128)(2,1)S(1)} %get-tuple-element.53), channel_id=1, source_target_pairs={{0,4},{2,6},{4,0},{6,2},{1,5},{3,7},{5,1},{7,3},{8,12},{10,14},{12... | collective-permute-start | bytes 983048 | tf_op jit(solution)/shard_map/ppermute | solution.py:338
  170.4 14.2 %collective-permute-start.19 = (bf16[40,4096]{1,0:T(8,128)(2,1)S(1)}, bf16[40,4096]{1,0:T(8,128)(2,1)S(1)}, u32[]{:S(2)}, u32[]{:S(2)}) collective-permute-start(bf16[40,4096]{1,0:T(8,128)(2,1)S(1)} %get-tuple-element.52), channel_id=1, source_target_pairs={{0,6},{2,0},{4,2},{6,4},{1,7},{3,1},{5,3},{7,5},{8,14},{10,8},{12,... | collective-permute-start | bytes 983048 | tf_op jit(solution)/shard_map/ppermute | solution.py:338
  (3 other events, 2.4 us)
